TPU v7x, 32 devices: a whole 2x2x4 slice. The times are simulated.
32 devices in a mesh: dp: 4 (over y, x), kv: 4 (over z), tp: 2 (over core).
Axes of the slice: x: 2, y: 2, z: 4, core: 2. Of those that a mesh axis runs over, the one named last changes fastest.
Arguments:
- tokens: bfloat16 [24, 4096], P('dp', 'kv'), may hold values from -64 to 64
- lengths: int32 [24], P('dp'), may hold values from 128 to 1024, as said below
- attn_gain: float32 [4096], P('kv'), may hold values from 0.1 to 1.9
- query_weight: bfloat16 [4096, 4096], P('kv', 'tp'), may hold values from -0.09375 to 0.09375
- key_weight: bfloat16 [4096, 256], P('kv', 'tp'), may hold values from -0.1875 to 0.1875
- value_weight: bfloat16 [4096, 256], P('kv', 'tp'), may hold values from -0.09375 to 0.09375
- forget_weight: bfloat16 [4096, 4], replicated, may hold values from -0.25 to 0.25
- forget_offset: float32 [4], P('tp'), may hold values from -6 to 0
- cache_keys: bfloat16 [24, 1024, 256], P('dp', 'kv', 'tp'), may hold values from -1600 to 1600
- cache_values: bfloat16 [24, 1024, 256], P('dp', 'kv', 'tp'), may hold values from -6 to 6
- gate_sum: float32 [24, 4, 1024], P('dp', 'tp', 'kv'), may hold values from -82 to 0
- out_weight: bfloat16 [4096, 4096], P('tp', 'kv'), may hold values from -0.1875 to 0.1875
- mlp_gain: float32 [4096], replicated, may hold values from 0.1 to 1.9
- up_weight: bfloat16 [4096, 16384], P(None, ('kv', 'tp')), may hold values from -0.09375 to 0.09375
- down_weight: bfloat16 [16384, 4096], P(('kv', 'tp')), may hold values from -0.0625 to 0.0625
Outputs:
- mixed: bfloat16 [24, 4096], P('dp', ('kv', 'tp'))
Inputs may be any that keep to these rules, and one draw needn't show every extreme that they name: `lengths`: in every draw some sequence has all 1024 positions cached.
All inputs are finite; a program needn't handle non-finite values.
Results may differ from a plain program's by a relative error of at most 0.023.
Values may be sent and summed in bfloat16 or wider, within the bound.
No kernel may reach another device: no remote copies, remote signals or barrier semaphores. Data moves between devices by JAX's collectives and lax.ppermute only.
A program may use at most 128 MiB of HBM per device.

v0:
```python
import jax
import jax.numpy as jnp
from jax import lax
from jax.sharding import PartitionSpec as P

D = 4096
HEADS = 64
HD = 64
KEY_VALUE_HEADS = 4


epsilon = 1e-06
floor_score = -1e30


def combined_all(x, axis, combine):
    everything = jax.tree.map(
        lambda part, kind: lax.all_gather(part.astype(kind), axis),
        x,
        (jnp.bfloat16, jnp.bfloat16, jnp.bfloat16),
    )

    def take(k):
        return jax.tree.map(lambda part, own: part[k].astype(own.dtype), everything, x)

    return lax.fori_loop(
        1, lax.axis_size(axis), lambda k, so_far: combine(so_far, take(k)), take(0)
    )


def combine_parts(earlier, later):
    first_top, first_total, first_values = earlier
    second_top, second_total, second_values = later
    merged_top = jnp.maximum(first_top, second_top)
    first_scale = jnp.exp(first_top - merged_top)
    second_scale = jnp.exp(second_top - merged_top)
    first_wide = jnp.repeat(first_scale, HD, axis=1)
    second_wide = jnp.repeat(second_scale, HD, axis=1)
    return (
        merged_top,
        first_total * first_scale + second_total * second_scale,
        first_values * first_wide + second_values * second_wide,
    )


def shards(
    tokens,
    lengths,
    attn_gain,
    query_weight,
    key_weight,
    value_weight,
    forget_weight,
    forget_offset,
    cache_keys,
    cache_values,
    gate_sum,
    out_weight,
    mlp_gain,
    up_weight,
    down_weight,
):
    row_count = tokens.shape[0]
    feature_cols = tokens.shape[1]
    kv_place = lax.axis_index("kv")
    tp_place = lax.axis_index("tp")
    local_heads = key_weight.shape[1] // HD
    group_size = HEADS // KEY_VALUE_HEADS
    token_rows = tokens.astype(jnp.float32)
    scaled_rows = (token_rows * attn_gain[None, :]).astype(jnp.bfloat16)
    square_part = jnp.sum(token_rows * token_rows, axis=1)
    query_part = jnp.dot(scaled_rows, query_weight, preferred_element_type=jnp.float32)
    key_part = jnp.dot(scaled_rows, key_weight, preferred_element_type=jnp.float32)
    value_part = jnp.dot(scaled_rows, value_weight, preferred_element_type=jnp.float32)
    gate_rows = lax.dynamic_slice(
        forget_weight,
        (kv_place * feature_cols, tp_place * local_heads),
        (feature_cols, local_heads),
    )
    forget_part = jnp.dot(scaled_rows, gate_rows, preferred_element_type=jnp.float32)
    query_sum, key_sum, value_sum, forget_sum, square_sum = lax.psum(
        (query_part, key_part, value_part, forget_part, square_part), "kv"
    )
    row_scale = lax.rsqrt(square_sum / D + epsilon)[:, None]
    queries = (query_sum * row_scale).astype(jnp.bfloat16)
    new_key = (key_sum * row_scale).astype(jnp.bfloat16)
    new_value = (value_sum * row_scale).astype(jnp.bfloat16)
    log_forget = jax.nn.log_sigmoid(forget_sum * row_scale + forget_offset[None, :])
    positions_here = cache_keys.shape[1]
    key_heads = cache_keys.reshape(row_count, positions_here, local_heads, HD)
    value_heads = cache_values.reshape(row_count, positions_here, local_heads, HD)
    query_heads = queries.reshape(row_count, local_heads, group_size, HD)
    scores = jnp.einsum(
        "skgd,spkd->skgp", query_heads, key_heads, preferred_element_type=jnp.float32
    ) * HD ** (-0.5)
    scores = scores + gate_sum[:, :, None, :] + log_forget[:, :, None, None]
    cache_pos = kv_place * positions_here + jnp.arange(positions_here)
    active_mask = (cache_pos[None, :] < lengths[:, None])[:, None, None, :]
    local_top = jnp.max(jnp.where(active_mask, scores, floor_score), axis=3)
    weights = jnp.where(active_mask, jnp.exp(scores - local_top[..., None]), 0.0)
    local_total = jnp.sum(weights, axis=3)
    local_values = jnp.einsum(
        "skgp,spkd->skgd",
        weights.astype(jnp.bfloat16),
        value_heads,
        preferred_element_type=jnp.float32,
    )
    head_cols = local_heads * group_size
    merged_top, merged_total, merged_values = combined_all(
        (
            local_top.reshape(row_count, head_cols),
            local_total.reshape(row_count, head_cols),
            local_values.reshape(row_count, head_cols * HD),
        ),
        "kv",
        combine_parts,
    )
    own_score = jnp.einsum(
        "skgd,skd->skg",
        query_heads,
        new_key.reshape(row_count, local_heads, HD),
        preferred_element_type=jnp.float32,
    ).reshape(row_count, head_cols) * HD ** (-0.5)
    final_top = jnp.maximum(merged_top, own_score)
    past_scale = jnp.exp(merged_top - final_top)
    own_weight = jnp.exp(own_score - final_top)
    totals = merged_total * past_scale + own_weight
    own_rounded = lax.optimization_barrier(own_weight.astype(jnp.bfloat16)).astype(jnp.float32)
    own_values = jnp.broadcast_to(
        new_value.astype(jnp.float32).reshape(row_count, local_heads, 1, HD),
        (row_count, local_heads, group_size, HD),
    ).reshape(row_count, head_cols * HD)
    weighted = (
        merged_values * jnp.repeat(past_scale, HD, axis=1)
        + jnp.repeat(own_rounded, HD, axis=1) * own_values
    )
    attended = (weighted / jnp.repeat(totals, HD, axis=1)).astype(jnp.bfloat16)
    partial_out = jnp.dot(attended, out_weight, preferred_element_type=jnp.float32)
    head_sum = lax.psum(partial_out.astype(jnp.bfloat16), "tp").astype(jnp.float32)
    mid_cols = (token_rows + head_sum).astype(jnp.bfloat16)
    mid_rows = lax.all_gather(mid_cols, "kv", axis=1, tiled=True)
    mid_wide = mid_rows.astype(jnp.float32)
    normed_mid = (
        mid_wide
        * mlp_gain[None, :]
        * lax.rsqrt(jnp.mean(mid_wide * mid_wide, axis=1, keepdims=True) + epsilon)
    ).astype(jnp.bfloat16)
    hidden = jnp.square(
        jax.nn.relu(jnp.dot(normed_mid, up_weight, preferred_element_type=jnp.float32))
    ).astype(jnp.bfloat16)
    mixer_term = jnp.dot(hidden, down_weight, preferred_element_type=jnp.float32)
    kv_count = lax.axis_size("kv")
    tp_count = lax.axis_size("tp")
    block_cols = mixer_term.shape[1] // (kv_count * tp_count)
    reordered = (
        mixer_term.reshape(row_count, kv_count, tp_count, block_cols)
        .transpose(0, 2, 1, 3)
        .reshape(row_count, kv_count * tp_count * block_cols)
    )
    pair_share = lax.psum_scatter(
        reordered.astype(jnp.bfloat16), "tp", scatter_dimension=1, tiled=True
    ).astype(jnp.float32)
    mixer_share = lax.psum_scatter(pair_share, "kv", scatter_dimension=1, tiled=True)
    out_cols = mixer_share.shape[1]
    start_col = (kv_place * tp_count + tp_place) * out_cols
    mid_share = lax.dynamic_slice_in_dim(mid_wide, start_col, out_cols, 1)
    return (mid_share + mixer_share).astype(jnp.bfloat16)


def solution(mesh):
    placed = (
        P("dp", "kv"),
        P("dp"),
        P("kv"),
        P("kv", "tp"),
        P("kv", "tp"),
        P("kv", "tp"),
        P(),
        P("tp"),
        P("dp", "kv", "tp"),
        P("dp", "kv", "tp"),
        P("dp", "tp", "kv"),
        P("tp", "kv"),
        P(),
        P(None, ("kv", "tp")),
        P(("kv", "tp"), None),
    )
    return jax.shard_map(
        shards, mesh=mesh, in_specs=placed, out_specs=P("dp", ("kv", "tp")), check_vma=False
    )
```

profile of v0, /device:TPU:0, one launch (start us, length us, event | category | flops | bytes accessed | tf_op | source)
XLA Modules:
  0.0 151.1 jit_solution(10252514063055072850)
XLA Ops:
  6.6 0.9 fusion.20
  7.4 2.9 %fusion.30 = f32[6,2048]{1,0:T(8,128)S(1)} fusion(bf16[1024,2048]{1,0:T(8,128)(2,1)} %param.20, bf16[6,1024]{1,0:T(8,128)(2,1)} %param.17, f32[1024]{0:T(1024)} %param.19), kind=kOutput, calls=%fused_computation.47 | convolution fusion | flops 25184256 | bytes 4259840 | tf_op jit(solution)/shard_map/dot_general | solution.py:72
  10.3 0.9 fusion.24
  11.2 1.1 fusion.26
  12.3 0.9 fusion.28
  13.3 22.1 %all-reduce = (f32[6,2048]{1,0:T(8,128)S(1)}, f32[6]{0:T(128)S(1)}, f32[6,128]{1,0:T(8,128)S(1)}, f32[6,2]{0,1:T(2,128)S(1)}, f32[6,128]{1,0:T(8,128)S(1)}) all-reduce(f32[6,2048]{1,0:T(8,128)S(1)} %fusion.30, f32[6]{0:T(128)S(1)} %fusion.20, f32[6,128]{1,0:T(8,128)S(1)} %fusion.26, ...), channel_id=1, replica_groups=mesh['dp'=4,'kv'=4,'tp'=2] {'kv'}, use_global_device_ids=true, to_apply=%region_0.0 | all-reduce | flops 13842 | bytes 110736 | tf_op jit(solution)/shard_map/psum | solution.py:81
  35.4 0.1 reshape.143
  35.5 0.7 fusion.39
  36.3 0.1 copy.25
  36.4 1.2 copy.24
  37.5 1.2 copy.26
  38.7 0.7 broadcast_compare_fusion
  39.4 1.0 select_reduce_fusion
  40.4 0.2 fusion.8
  40.6 0.3 convolution_convert_fusion.1
  40.9 0.1 convert_element_type.173
  41.0 13.6 %all_gather.17 = bf16[4,6,2048]{2,1,0:T(8,128)(2,1)S(1)} all-gather(bf16[1,6,2048]{2,1,0:T(8,128)(2,1)S(1)} %convert_element_type.173), channel_id=1, replica_groups=mesh['dp'=4,'kv'=4,'tp'=2] {'kv'}, dimensions={0}, use_global_device_ids=true | all-gather | bytes 122880 | tf_op jit(solution)/shard_map/all_gather | solution.py:18
  54.6 0.1 convert_element_type.168
  54.7 11.9 %all_gather.16 = bf16[4,6,32]{2,1,0:T(8,128)(2,1)S(1)} all-gather(bf16[1,6,32]{2,1,0:T(8,128)(2,1)S(1)} %convert_element_type.168), channel_id=1, replica_groups=mesh['dp'=4,'kv'=4,'tp'=2] {'kv'}, dimensions={0}, use_global_device_ids=true | all-gather | bytes 1920 | tf_op jit(solution)/shard_map/all_gather | solution.py:18
  66.6 0.1 convert_element_type.164
  66.7 11.9 %all_gather.15 = bf16[4,6,32]{2,1,0:T(8,128)(2,1)S(1)} all-gather(bf16[1,6,32]{2,1,0:T(8,128)(2,1)S(1)} %convert_element_type.164), channel_id=1, replica_groups=mesh['dp'=4,'kv'=4,'tp'=2] {'kv'}, dimensions={0}, use_global_device_ids=true | all-gather | bytes 1920 | tf_op jit(solution)/shard_map/all_gather | solution.py:18
  78.6 1.3 while.19
  78.7 0.1 broadcast_in_dim.93
  78.8 0.1 reshape.164
  78.9 0.1 reshape.165
  79.2 0.1 reshape.164
  79.4 0.1 reshape.165
  79.6 0.1 reshape.164
  79.8 0.1 reshape.165
  80.0 0.1 reshape.161
  80.1 0.1 fusion.44
  80.2 0.1 mul.155
  80.3 0.1 broadcast_in_dim.71
  80.4 0.1 reshape.147
  80.5 0.1 broadcast_in_dim.72
  80.6 0.1 reshape.148
  80.8 0.1 reshape.150
  81.0 0.1 reshape.149
  81.1 2.8 %convolution_convert_fusion.2 = bf16[6,1024]{1,0:T(8,128)(2,1)S(1)} fusion(bf16[2048,1024]{1,0:T(8,128)(2,1)} %param.28, f32[6,2048]{1,0:T(8,128)S(1)} %reshape.150, f32[6,2048]{1,0:T(8,128)S(1)} %reshape.148, f32[6,2048]{1,0:T(8,128)S(1)} %reshape.149, f32[6,2048]{1,0:T(8,128)S(1)} %get-tuple-element.183, f32[6,2048]{1,0:T(8,128)S(1)} %reshape.147), kind=kOutput, calls=%fused_computation.16 | convolution fusion | flops 25233408 | bytes 4452352 | tf_op jit(solution)/shard_map/dot_general | solution.py:138
  83.9 3.4 %psum.47 = bf16[6,1024]{1,0:T(8,128)(2,1)S(1)} all-reduce(bf16[6,1024]{1,0:T(8,128)(2,1)S(1)} %convolution_convert_fusion.2), channel_id=1, replica_groups=mesh['dp'=4,'kv'=4,'tp'=2] {'tp'}, use_global_device_ids=true, to_apply=%region_10.11 | all-reduce | flops 6144 | bytes 24576 | tf_op jit(solution)/shard_map/psum | solution.py:139
  87.3 13.1 %all_gather.18 = bf16[6,4096]{1,0:T(8,128)(2,1)S(1)} all-gather(bf16[6,1024]{1,0:T(8,128)(2,1)S(1)} %fusion.21), channel_id=1, replica_groups=mesh['dp'=4,'kv'=4,'tp'=2] {'kv'}, dimensions={1}, use_global_device_ids=true | all-gather | bytes 61440 | tf_op jit(solution)/shard_map/all_gather | solution.py:141
  100.4 0.1 multiply_reduce_fusion
  100.6 12.9 %convolution_convert_fusion = bf16[6,4096]{1,0:T(8,128)(2,1)S(1)} fusion(bf16[2048,4096]{1,0:T(8,128)(2,1)} %param.31, bf16[4096,2048]{1,0:T(8,128)(2,1)} %param.30, f32[6]{0:T(128)S(1)} %add_rsqrt_fusion, f32[4096]{0:T(1024)S(1)} %copy-done.2, bf16[6,4096]{1,0:T(8,128)(2,1)S(1)} %all_gather.18), kind=kOutput, calls=%fused_computation.8 | convolution fusion | flops 201486336 | bytes 33669144 | tf_op jit(solution)/shard_map/dot_general | solution.py:151
  113.6 0.7 convert_element_type.190
  114.3 5.9 %reduce-scatter.3.cloned.1.call-done = bf16[6,2048]{1,0:T(8,128)(2,1)} async-done(((bf16[6,4096]{1,0:T(8,128)(2,1)}), bf16[6,2048]{1,0:T(8,128)(2,1)}) %reduce-scatter.3.cloned.1.call-update) | async-done | bytes 24592 | tf_op jit(solution)/shard_map/reduce_scatter | solution.py:160
  120.2 1.4 convert_element_type.191
  121.6 21.3 %reduce-scatter.5.cloned.1.call-done = f32[6,512]{1,0:T(8,128)} async-done(((f32[6,2048]{1,0:T(8,128)}), f32[6,512]{1,0:T(8,128)}) %reduce-scatter.5.cloned.1.call-update) | async-done | bytes 12304 | tf_op jit(solution)/shard_map/reduce_scatter | solution.py:163
  142.9 1.3 add_convert_fusion
  (39 shorter events, 1.1 us)
Async XLA Ops:
  6.5 3.8 %copy-start = (bf16[1024,128]{1,0:T(8,128)(2,1)S(1)}, bf16[1024,128]{1,0:T(8,128)(2,1)}, u32[]{:S(2)}) copy-start(bf16[1024,128]{1,0:T(8,128)(2,1)} %param.22) | copy-start | bytes 786436
  6.5 80.7 %copy-start.1 = (bf16[6,1024]{1,0:T(8,128)(2,1)S(1)}, bf16[6,1024]{1,0:T(8,128)(2,1)}, u32[]{:S(2)}) copy-start(bf16[6,1024]{1,0:T(8,128)(2,1)} %param.17) | copy-start | bytes 36868
  6.5 94.1 %copy-start.2 = (f32[4096]{0:T(1024)S(1)}, f32[4096]{0:T(1024)}, u32[]{:S(2)}) copy-start(f32[4096]{0:T(1024)} %param.29) | copy-start | bytes 49156
  6.5 113.7 %reduce-scatter.3.cloned.1.call-start = ((), (), s32[]{:S(2)}) async-start(), calls=%async_computation.2 | async-start | bytes 98304 | tf_op jit(solution)/shard_map/reduce_scatter | solution.py:160
  114.3 28.6 %reduce-scatter.5.cloned.1.call-start = ((), (), s32[]{:S(2)}) async-start(), calls=%async_computation.3 | async-start | bytes 81920 | tf_op jit(solution)/shard_map/reduce_scatter | solution.py:163
Sparse Core Ops, SparseCore 0:
  114.4 5.7 reduce-scatter.2
  122.5 20.4 reduce-scatter.4
where the time goes:
time: 152 us; the launch traced here: 151 us
  blocking collectives  76 us (50%)
  waiting for transfers between devices  27.2 us (18%)
  matrix products  22.9 us (15%)
  between operations  13.6 us (9%)
  other arithmetic  5.77 us (4%)
  local copies, waits for them, and re-layouts  5.52 us (4%)
    all_gather x3, blocking collectives, combined_all(): lax.all_gather(part.astype(kind), axis)  37.4 us
    psum x1, blocking collectives, shards(): lax.psum((query_part, key_part, value_part, forget_part, square_part), 'kv')  22.1 us
    reduce_scatter x1, waiting for transfers between devices, shards(): lax.psum_scatter(pair_share, 'kv', scatter_dimension=1, tiled=True)  21.3 us
    all_gather x1, blocking collectives, shards(): mid_rows = lax.all_gather(mid_cols, 'kv', axis=1, tiled=True)  13.1 us
    dot_general x1, matrix products, shards(): jnp.dot(hidden, down_weight, preferred_element_type=jnp.float32)  12.9 us
    reduce_scatter x1, waiting for transfers between devices, shards(): lax.psum_scatter(reordered.astype(jnp.bfloat16), 'tp', scatter_dimension=...  5.88 us
    psum x1, blocking collectives, shards(): lax.psum(partial_out.astype(jnp.bfloat16), 'tp').astype(jnp.float32)  3.36 us
  transfers between devices with their start and end apart: 2, of which 2 were waited for; matrix products, arithmetic and copies ran while one was open for 0% of the time, Pallas kernels for 0%

commit v1 on v0

--- a/solution.py
+++ b/solution.py
@@ -1,6 +1,9 @@
+import functools
 import jax
 import jax.numpy as jnp
 from jax import lax
+from jax.experimental import pallas as pl
+from jax.experimental.pallas import tpu as pltpu
 from jax.sharding import PartitionSpec as P
 
 D = 4096
@@ -167,6 +170,500 @@
     return (mid_share + mixer_share).astype(jnp.bfloat16)
 
 
+LANES = 128
+SUBLANES = 8
+VMEM = pltpu.VMEM
+HBM = pltpu.HBM
+f32 = jnp.float32
+bf16 = jnp.bfloat16
+in_vmem = pl.BlockSpec(memory_space=pltpu.VMEM)
+in_smem = pl.BlockSpec(memory_space=pltpu.SMEM)
+in_hbm = pl.BlockSpec(memory_space=pltpu.HBM)
+anywhere = pl.BlockSpec(memory_space=pl.ANY)
+
+
+def call(kernel, outs, in_specs, args, scratch=(), megabytes=8, weight_bytes=0, name=None):
+    many = isinstance(outs, (list, tuple))
+    return pl.pallas_call(
+        kernel,
+        out_shape=outs,
+        in_specs=in_specs,
+        out_specs=[in_vmem] * len(outs) if many else in_vmem,
+        scratch_shapes=list(scratch),
+        compiler_params=pltpu.CompilerParams(vmem_limit_bytes=megabytes * 1024 * 1024),
+        cost_estimate=pl.CostEstimate(
+            flops=12 * max(weight_bytes, 1 << 16),
+            bytes_accessed=max(weight_bytes, 1 << 16),
+            transcendentals=0,
+        ),
+        name=name,
+    )(*args)
+
+
+def pinned(x, space):
+    return pltpu.with_memory_space_constraint(x, space)
+
+
+def round_up(n, m):
+    return -(-n // m) * m
+
+
+def lane_index(rows):
+    return lax.broadcasted_iota(jnp.int32, (rows, LANES), 1)
+
+
+def project_kernel(
+    tokens_hbm,
+    gain_hbm,
+    query_hbm,
+    key_hbm,
+    value_hbm,
+    forget_hbm,
+    part_ref,
+    tokens,
+    gain,
+    query,
+    key,
+    value,
+    forget,
+    stage,
+    sems,
+):
+    rows, feats = tokens.shape
+    chunks = query.shape[0]
+    depth = query.shape[1]
+    kv_place = lax.axis_index("kv")
+    start = pl.multiple_of(kv_place * feats, feats)
+    copies = [
+        pltpu.make_async_copy(tokens_hbm, tokens, sems.at[0]),
+        pltpu.make_async_copy(gain_hbm, gain, sems.at[1]),
+        pltpu.make_async_copy(forget_hbm.at[pl.ds(start, feats), :], forget, sems.at[2]),
+        pltpu.make_async_copy(key_hbm, key, sems.at[3]),
+        pltpu.make_async_copy(value_hbm, value, sems.at[4]),
+    ]
+    streams = [
+        pltpu.make_async_copy(
+            query_hbm.at[pl.ds(i * depth, depth), :], query.at[i], sems.at[5 + i]
+        )
+        for i in range(chunks)
+    ]
+    for copy in copies[:2]:
+        copy.start()
+    for copy in streams:
+        copy.start()
+    for copy in copies[2:]:
+        copy.start()
+    for copy in copies[:2]:
+        copy.wait()
+    token_rows = tokens[...].astype(f32)
+    scaled = (token_rows * gain[...]).astype(bf16)
+    squares = jnp.sum(token_rows * token_rows, axis=1, keepdims=True)
+    total = None
+    for i in range(chunks):
+        streams[i].wait()
+        term = jnp.dot(
+            scaled[:, i * depth : (i + 1) * depth], query[i], preferred_element_type=f32
+        )
+        total = term if total is None else total + term
+    for copy in copies[2:]:
+        copy.wait()
+    key_part = jnp.dot(scaled, key[...], preferred_element_type=f32)
+    value_part = jnp.dot(scaled, value[...], preferred_element_type=f32)
+    forget_part = jnp.dot(scaled, forget[...], preferred_element_type=f32)
+    heads = forget_part.shape[1]
+    lane = lane_index(rows)
+    extra = jnp.where(lane == heads, squares, 0.0)
+    for j in range(heads):
+        extra = jnp.where(lane == j, forget_part[:, j : j + 1], extra)
+    high = extra.astype(bf16).astype(f32)
+    low = extra - high
+    extra = high + pltpu.roll(low, LANES // 2, axis=1)
+    stage[...] = jnp.zeros(stage.shape, f32)
+    tiles = total.shape[1] // LANES
+    for c in range(tiles):
+        stage[c * rows : (c + 1) * rows, :] = total[:, c * LANES : (c + 1) * LANES]
+    for j, block in enumerate((key_part, value_part, extra)):
+        stage[(tiles + j) * rows : (tiles + j + 1) * rows, :] = block
+    part_ref[...] = stage[...].astype(bf16)
+
+
+def hold_kernel(count, *refs):
+    sources = refs[1 : 1 + count]
+    targets = refs[1 + count : 1 + 2 * count]
+    sems = refs[1 + 2 * count]
+    copies = [
+        pltpu.make_async_copy(s, t, sems.at[i])
+        for i, (s, t) in enumerate(zip(sources, targets))
+    ]
+    for copy in copies:
+        copy.start()
+    for copy in copies:
+        copy.wait()
+
+
+def hold(after, arrays, name):
+    outs = [pltpu.VMEM(a.shape, a.dtype) for a in arrays]
+    size = sum(a.size * a.dtype.itemsize for a in arrays)
+    return call(
+        functools.partial(hold_kernel, len(arrays)),
+        outs,
+        [anywhere] + [in_hbm] * len(arrays),
+        [after] + [pinned(a, HBM) for a in arrays],
+        scratch=[pltpu.SemaphoreType.DMA((len(arrays),))],
+        megabytes=1,
+        weight_bytes=size,
+        name=name,
+    )
+
+
+def hold_rows_kernel(first, count, pieces, _, source, target, sems):
+    depth = count // pieces
+    copies = [
+        pltpu.make_async_copy(
+            source.at[pl.ds(first + i * depth, depth), :],
+            target.at[pl.ds(i * depth, depth), :],
+            sems.at[i],
+        )
+        for i in range(pieces)
+    ]
+    for copy in copies:
+        copy.start()
+    for copy in copies:
+        copy.wait()
+
+
+def hold_rows(after, array, first, count, name):
+    pieces = 4
+    return call(
+        functools.partial(hold_rows_kernel, first, count, pieces),
+        pltpu.VMEM((count, array.shape[1]), array.dtype),
+        [anywhere, in_hbm],
+        [after, pinned(array, HBM)],
+        scratch=[pltpu.SemaphoreType.DMA((pieces,))],
+        megabytes=1,
+        weight_bytes=count * array.shape[1] * array.dtype.itemsize,
+        name=name,
+    )
+
+
+def attend_kernel(
+    peers, rows, lengths, offset, keys, values, gates, *refs
+):
+    parts = refs[:peers]
+    sent_ref, stage = refs[peers:]
+    positions = keys.shape[1]
+    kv_place = lax.axis_index("kv")
+    tp_place = lax.axis_index("tp")
+    summed = parts[0][...].astype(f32)
+    for part in parts[1:]:
+        summed = summed + part[...].astype(f32)
+    stage[...] = summed
+    tiles = HEADS // lax.axis_size("tp") * HD // LANES
+    half = tiles // 2
+    extra = stage[(tiles + 2) * rows : (tiles + 3) * rows, :]
+    extra = extra + pltpu.roll(extra, LANES // 2, axis=1)
+    scale = lax.rsqrt(extra[:, KEY_VALUE_HEADS : KEY_VALUE_HEADS + 1] / D + epsilon)
+    gate_in = extra * scale
+    lane_row = lax.broadcasted_iota(jnp.int32, (tiles, LANES), 1)
+    tile_row = lax.broadcasted_iota(jnp.int32, (tiles, LANES), 0)
+    low_lane = lane_row < HD
+    low_tile = tile_row < half
+    mine = low_lane == low_tile
+    wide_tile = lax.broadcasted_iota(jnp.int32, (tiles, positions), 0) < half
+    place = kv_place * positions + lax.broadcasted_iota(jnp.int32, (2 * tiles, positions), 1)
+    owner = kv_place == 0
+    stats = jnp.zeros((tiles, LANES), f32)
+    for b in range(rows):
+        row_scale = scale[b : b + 1, :]
+        tile = (stage[pl.ds(b, tiles, stride=rows), :] * row_scale).astype(bf16).astype(f32)
+        turned = pltpu.roll(tile, HD, axis=1)
+        even = jnp.where(low_tile, tile, turned)
+        odd = jnp.where(low_tile, turned, tile)
+        even = jnp.where(mine, even, 0.0)
+        odd = jnp.where(mine, odd, 0.0)
+        query = jnp.concatenate([even, odd], axis=0)
+        new_key = (stage[tiles * rows + b : tiles * rows + b + 1, :] * row_scale).astype(bf16)
+        new_value = (
+            stage[(tiles + 1) * rows + b : (tiles + 1) * rows + b + 1, :] * row_scale
+        ).astype(bf16)
+        scores = lax.dot_general(
+            query.astype(bf16),
+            keys[b],
+            (((1,), (1,)), ((), ())),
+            preferred_element_type=f32,
+        ) * HD ** (-0.5)
+        both = []
+        for g in range(2):
+            column = tp_place * 2 + g
+            picked = jnp.sum(
+                jnp.where(
+                    lax.broadcasted_iota(jnp.int32, (1, LANES), 1) == column,
+                    gate_in[b : b + 1, :],
+                    0.0,
+                ),
+                axis=1,
+                keepdims=True,
+            )
+            raw = picked + offset[g]
+            log_forget = jnp.minimum(raw, 0.0) - jnp.log1p(jnp.exp(-jnp.abs(raw)))
+            both.append(gates[b, g : g + 1, :] + log_forget)
+        bias = jnp.where(wide_tile, both[0], both[1])
+        scores = scores + jnp.concatenate([bias, bias], axis=0)
+        live = place < lengths[b]
+        scores = jnp.where(live, scores, floor_score)
+        own = jnp.sum(query * new_key.astype(f32), axis=1, keepdims=True) * HD ** (-0.5)
+        own = jnp.where(owner, own, floor_score)
+        top = jnp.maximum(jnp.max(scores, axis=1, keepdims=True), own)
+        top_high = top.astype(bf16).astype(f32)
+        top_low = (top - top_high).astype(bf16).astype(f32)
+        top = top_high + top_low
+        weights = jnp.where(live, jnp.exp(scores - top), 0.0)
+        own_weight = jnp.where(owner, jnp.exp(own - top), 0.0)
+        total = jnp.sum(weights, axis=1, keepdims=True) + own_weight
+        total_high = total.astype(bf16).astype(f32)
+        total_low = total - total_high
+        summed_values = jnp.dot(weights.astype(bf16), values[b], preferred_element_type=f32)
+        summed_values = summed_values + own_weight.astype(bf16).astype(f32) * new_value.astype(f32)
+        even = summed_values[:tiles]
+        odd = summed_values[tiles:]
+        placed_even = jnp.where(low_tile, even, pltpu.roll(even, HD, axis=1))
+        placed_odd = jnp.where(low_tile, pltpu.roll(odd, HD, axis=1), odd)
+        sent_ref[b * tiles : (b + 1) * tiles, :] = jnp.where(
+            low_lane, placed_even, placed_odd
+        ).astype(bf16)
+        for j, column in enumerate((top_high, top_low, total_high, total_low)):
+            for parity in range(2):
+                stats = jnp.where(
+                    lane_row == j * (LANES // 4) + 2 * b + parity,
+                    column[parity * tiles : (parity + 1) * tiles],
+                    stats,
+                )
+    sent_ref[rows * tiles :, :] = stats.astype(bf16)
+
+
+def output_kernel(peers, rows, weight, tokens, _, *refs):
+    parts = refs[:peers]
+    partial_ref, kept_ref, stage = refs[peers:]
+    tiles = parts[0].shape[0] // (rows + 1)
+    quarter = LANES // 4
+    tops, totals = [], []
+    for part in parts:
+        stats = part[rows * tiles :, :].astype(f32)
+        tops.append(stats + pltpu.roll(stats, LANES - quarter, axis=1))
+        totals.append(
+            pltpu.roll(stats, LANES - 2 * quarter, axis=1)
+            + pltpu.roll(stats, LANES - 3 * quarter, axis=1)
+        )
+    top = functools.reduce(jnp.maximum, tops)
+    scales = [jnp.exp(t - top) for t in tops]
+    total = functools.reduce(jnp.add, [t * s for t, s in zip(totals, scales)])
+    shares = [s / total for s in scales]
+    low_lane = lane_index(tiles) < HD
+    for b in range(rows):
+        mixed = None
+        for part, share in zip(parts, shares):
+            factor = jnp.where(
+                low_lane, share[:, 2 * b : 2 * b + 1], share[:, 2 * b + 1 : 2 * b + 2]
+            )
+            term = part[b * tiles : (b + 1) * tiles, :].astype(f32) * factor
+            mixed = term if mixed is None else mixed + term
+        stage[b * tiles : (b + 1) * tiles, :] = mixed
+    attended = jnp.concatenate(
+        [stage[pl.ds(c, rows, stride=tiles), :] for c in range(tiles)], axis=1
+    ).astype(bf16)
+    partial = jnp.dot(attended, weight[...], preferred_element_type=f32).astype(bf16)
+    partial_ref[...] = partial
+    kept_ref[...] = tokens[...].astype(f32) + partial.astype(f32)
+
+
+def mixer_kernel(
+    peers, gain, up_low, up_high, down_hbm, *refs
+):
+    mids = refs[:peers]
+    kept_ref, sent_ref, down, normed, spread, sems = refs[peers:]
+    rows, width = mids[0].shape
+    chunks, depth = down.shape[:2]
+    kv_place = lax.axis_index("kv")
+    tp_place = lax.axis_index("tp")
+    streams = [
+        pltpu.make_async_copy(
+            down_hbm.at[pl.ds(i * depth, depth), :], down.at[i], sems.at[i]
+        )
+        for i in range(chunks)
+    ]
+    for copy in streams:
+        copy.start()
+    wides = [m[...].astype(f32) for m in mids]
+    squares = functools.reduce(
+        jnp.add, [jnp.sum(w * w, axis=1, keepdims=True) for w in wides]
+    )
+    scale = lax.rsqrt(squares / D + epsilon)
+    for k in range(peers):
+        source = kv_place ^ k
+        normed[source] = wides[k] * gain[source] * scale
+    half = peers // 2
+    hidden = None
+    for j in range(peers):
+        up = up_low if j < half else up_high
+        first = (j % half) * width
+        term = jnp.dot(
+            normed[j].astype(bf16), up[first : first + width, :], preferred_element_type=f32
+        )
+        hidden = term if hidden is None else hidden + term
+    hidden = jnp.square(jnp.maximum(hidden, 0.0)).astype(bf16)
+    total = None
+    for i in range(chunks):
+        streams[i].wait()
+        term = jnp.dot(
+            hidden[:, i * depth : (i + 1) * depth], down[i], preferred_element_type=f32
+        )
+        total = term if total is None else total + term
+    blocks = spread.shape[0]
+    cols = spread.shape[2]
+    for q in range(blocks):
+        spread[q] = total[:, q * cols : (q + 1) * cols]
+    for k in range(peers):
+        target = 2 * (kv_place ^ k)
+        kept_ref[k] = spread[target + tp_place]
+        sent_ref[k] = spread[target + 1 - tp_place].astype(bf16)
+    for half_place in range(2):
+
+        @pl.when(tp_place == half_place)
+        def _():
+            kept_ref[0] += mids[0][:, half_place * cols : (half_place + 1) * cols].astype(f32)
+
+
+def swap(x, axis, k):
+    return lax.ppermute(x, axis, [(i, i ^ k) for i in range(lax.axis_size(axis))])
+
+
+def shards_direct(
+    tokens,
+    lengths,
+    attn_gain,
+    query_weight,
+    key_weight,
+    value_weight,
+    forget_weight,
+    forget_offset,
+    cache_keys,
+    cache_values,
+    gate_sum,
+    out_weight,
+    mlp_gain,
+    up_weight,
+    down_weight,
+):
+    rows, feats = tokens.shape
+    peers = lax.axis_size("kv")
+    others = range(1, peers)
+    tiles = query_weight.shape[1] // LANES
+    chunks = 4
+    depth = feats // chunks
+    part_rows = round_up((tiles + 3) * rows, SUBLANES)
+    part = call(
+        project_kernel,
+        jax.ShapeDtypeStruct((part_rows, LANES), bf16),
+        [in_hbm] * 6,
+        [
+            pinned(x, HBM)
+            for x in (
+                tokens,
+                attn_gain.reshape(1, feats),
+                query_weight,
+                key_weight,
+                value_weight,
+                forget_weight,
+            )
+        ],
+        scratch=[
+            pltpu.VMEM((rows, feats), bf16),
+            pltpu.VMEM((1, feats), f32),
+            pltpu.VMEM((chunks, depth, query_weight.shape[1]), bf16),
+            pltpu.VMEM(key_weight.shape, bf16),
+            pltpu.VMEM(value_weight.shape, bf16),
+            pltpu.VMEM((feats, forget_weight.shape[1]), bf16),
+            pltpu.VMEM((part_rows, LANES), f32),
+            pltpu.SemaphoreType.DMA((5 + chunks,)),
+        ],
+        megabytes=12,
+        weight_bytes=query_weight.size * 2,
+        name="project",
+    )
+    parts = [part] + [swap(part, "kv", k) for k in others]
+    keys_held, values_held, gates_held, out_held, tokens_held = hold(
+        part, [cache_keys, cache_values, gate_sum, out_weight, tokens], "hold_caches"
+    )
+    sent = call(
+        functools.partial(attend_kernel, peers, rows),
+        jax.ShapeDtypeStruct(((rows + 1) * tiles, LANES), bf16),
+        [in_smem] * 2 + [in_vmem] * (3 + peers),
+        [lengths, forget_offset]
+        + [pinned(x, VMEM) for x in (keys_held, values_held, gates_held)]
+        + parts,
+        scratch=[pltpu.VMEM((part_rows, LANES), f32)],
+        megabytes=6,
+        name="attend",
+    )
+    sents = [sent] + [swap(sent, "kv", k) for k in others]
+    total_rows = up_weight.shape[0]
+    up_low = hold_rows(sent, up_weight, 0, total_rows // 2, "hold_low")
+    partial, kept = call(
+        functools.partial(output_kernel, peers, rows),
+        [
+            jax.ShapeDtypeStruct((rows, out_weight.shape[1]), bf16),
+            jax.ShapeDtypeStruct((rows, out_weight.shape[1]), f32),
+        ],
+        [in_vmem] * 2 + [anywhere] + [in_vmem] * peers,
+        [pinned(out_held, VMEM), pinned(tokens_held, VMEM), pinned(up_low, VMEM)] + sents,
+        scratch=[pltpu.VMEM((rows * tiles, LANES), f32)],
+        megabytes=6,
+        name="output",
+    )
+    mid = (kept + swap(partial, "tp", 1).astype(f32)).astype(bf16)
+    mids = [mid] + [swap(mid, "kv", k) for k in others]
+    up_high = hold_rows(mid, up_weight, total_rows // 2, total_rows // 2, "hold_high")
+    hidden_rows, model = down_weight.shape
+    pieces = 8
+    blocks = 2 * peers
+    cols = model // blocks
+    kept, crossing = call(
+        functools.partial(mixer_kernel, peers),
+        [
+            jax.ShapeDtypeStruct((peers, rows, cols), f32),
+            jax.ShapeDtypeStruct((peers, rows, cols), bf16),
+        ],
+        [in_vmem] * 3 + [in_hbm] + [in_vmem] * peers,
+        [
+            mlp_gain.reshape(peers, 1, model // peers),
+            pinned(up_low, VMEM),
+            pinned(up_high, VMEM),
+            pinned(down_weight, HBM),
+        ]
+        + mids,
+        scratch=[
+            pltpu.VMEM((pieces, hidden_rows // pieces, model), bf16),
+            pltpu.VMEM((peers, rows, model // peers), f32),
+            pltpu.VMEM((blocks, rows, cols), f32),
+            pltpu.SemaphoreType.DMA((pieces,)),
+        ],
+        megabytes=24,
+        weight_bytes=down_weight.size * 2,
+        name="mixer",
+    )
+    paired = kept + swap(crossing, "tp", 1).astype(f32)
+    shares = [swap(paired[k].astype(bf16), "kv", k) for k in others]
+    result = paired[0]
+    for share in shares:
+        result = result + share.astype(f32)
+    return result.astype(bf16)
+
+
+def direct_fits(mesh):
+    peers = mesh.shape["kv"]
+    return mesh.shape["tp"] == 2 and peers in (2, 4) and HD * 2 == LANES
+
+
 def solution(mesh):
     placed = (
         P("dp", "kv"),
@@ -186,5 +683,5 @@
         P(("kv", "tp"), None),
     )
     return jax.shard_map(
-        shards, mesh=mesh, in_specs=placed, out_specs=P("dp", ("kv", "tp")), check_vma=False
-    )
+        shards_direct if direct_fits(mesh) else shards, mesh=mesh, in_specs=placed, out_specs=P("dp", ("kv", "tp")), check_vma=False
+    )

time: 152 us -> 51.3 us (0.34)
  blocking collectives: 76 us -> 0 us
  matrix products: 22.9 us -> 0 us
  Pallas kernels: 0 us -> 22.4 us
  waiting for transfers between devices: 27.2 us -> 7.43 us
  starting transfers between devices: 0.04 us -> 18.3 us
  between operations: 13.6 us -> 0.14 us
  other arithmetic: 5.77 us -> 0.63 us
  local copies, waits for them, and re-layouts: 5.52 us -> 2.2 us
    all_gather x4 -> x0, blocking collectives: 50.6 us -> none  [the longest x3 37.4 us: combined_all(): lax.all_gather(part.astype(kind), axis)]
    reduce_scatter x2 -> x0, waiting for transfers between devices: 27.1 us -> none  [the longest x1 21.3 us: shards(): lax.psum_scatter(pair_share, 'kv', scatter_dimension=1, tiled=True)]
    psum x2 -> x0, blocking collectives: 25.4 us -> none  [the longest x1 22.1 us: shards(): lax.psum((query_part, key_part, value_part, forget_part, square_part), 'kv')]
    dot_general x9 -> x0, matrix products: 22.9 us -> none  [the longest x1 12.9 us: shards(): jnp.dot(hidden, down_weight, preferred_element_type=jnp.float32)]
    pallas_call x0 -> x7, Pallas kernels: none -> 22.4 us  [call(): pl.pallas_call(kernel, out_shape=outs, in_specs=in_specs, out_specs=[in_v...]
    ppermute x0 -> x14, starting transfers between devices: none -> 18.3 us  [swap(): lax.ppermute(x, axis, [(i, i ^ k) for i in range(lax.axis_size(axis))])]
    ppermute x0 -> x14, waiting for transfers between devices: none -> 7.43 us  [swap(): lax.ppermute(x, axis, [(i, i ^ k) for i in range(lax.axis_size(axis))])]
    convert_element_type x9 -> x2, other arithmetic: 2.81 us -> 0.62 us  [the longest x1 0.61 us: shards_direct(): return result.astype(bf16)]
  transfers between devices with their start and end apart: 2 -> 14, of which waited for: 2 -> 6; matrix products, arithmetic and copies ran while one was open for 0% -> 0% of each run, Pallas kernels for 0% -> 19%
where the time goes in v1:
time: 51.3 us; the launch traced here: 51 us
  Pallas kernels  22.4 us (44%)
  starting transfers between devices  18.3 us (36%)
  waiting for transfers between devices  7.43 us (14%)
  local copies, waits for them, and re-layouts  2.2 us (4%)
  other arithmetic  0.63 us (1%)
    pallas_call x7, Pallas kernels, call(): pl.pallas_call(kernel, out_shape=outs, in_specs=in_specs, out_specs=[in_v...  22.4 us
    ppermute x14, starting transfers between devices, swap(): lax.ppermute(x, axis, [(i, i ^ k) for i in range(lax.axis_size(axis))])  18.3 us
    ppermute x14, waiting for transfers between devices, swap(): lax.ppermute(x, axis, [(i, i ^ k) for i in range(lax.axis_size(axis))])  7.43 us
    unnamed x7, local copies, waits for them, and re-layouts  2.2 us
  transfers between devices with their start and end apart: 14, of which 6 were waited for; matrix products, arithmetic and copies ran while one was open for 0% of the time, Pallas kernels for 19%

profile of v1, /device:TPU:0, one launch (start us, length us, event | category | flops | bytes accessed | tf_op | source)
XLA Modules:
  0.0 51.0 jit_solution(10993461672254859254)
XLA Ops:
  0.0 0.0 copy-start.2
  0.0 0.0 copy-start.1
  0.0 2.2 %copy.16.forget_hbm = bf16[4096,4]{1,0:T(8,128)(2,1)} copy(bf16[4096,4]{0,1:T(4,128)(2,1)} %param.21) | data formatting | bytes 65536 | tf_op args[6]
  2.2 2.9 %project.1.refs_0_ = bf16[120,128]{1,0:T(8,128)(2,1)S(1)} custom-call(bf16[6,1024]{1,0:T(8,128)(2,1)} %refs_5_.1, f32[1,1024]{1,0:T(1,128)} %bitcast.19, bf16[1024,2048]{1,0:T(8,128)(2,1)} %query_hbm.1, bf16[1024,128]{1,0:T(8,128)(2,1)} %key_hbm.1, bf16[1024,128]{1,0:T(8,128)(2,1)} %value_hbm.1, bf16[4096,4]{1,0:T(8,128)(2,1)} %copy.16.forget_hbm), custom_call_target="tpu_custom_call" | custom-call | flops 50331648 | bytes 4194304 | tf_op jit(solution)/shard_map/project/pallas_call | solution.py:187
  5.1 5.1 %collective-permute-start.2 = (bf16[120,128]{1,0:T(8,128)(2,1)S(1)}, bf16[120,128]{1,0:T(8,128)(2,1)S(1)}, u32[]{:S(2)}, u32[]{:S(2)}) collective-permute-start(bf16[120,128]{1,0:T(8,128)(2,1)S(1)} %project.1.refs_0_), channel_id=1, source_target_pairs={{0,6},{2,4},{4,2},{6,0},{1,7},{3,5},{5,3},{7,1},{8,14},{10,12},{12... | collective-permute-start | bytes 92168 | tf_op jit(solution)/shard_map/ppermute | solution.py:537
  10.3 0.0 collective-permute-start.1
  10.3 0.6 %collective-permute-start = (bf16[120,128]{1,0:T(8,128)(2,1)S(1)}, bf16[120,128]{1,0:T(8,128)(2,1)S(1)}, u32[]{:S(2)}, u32[]{:S(2)}) collective-permute-start(bf16[120,128]{1,0:T(8,128)(2,1)S(1)} %project.1.refs_0_), channel_id=1, source_target_pairs={{0,2},{2,0},{4,6},{6,4},{1,3},{3,1},{5,7},{7,5},{8,10},{10,8},{12,... | collective-permute-start | bytes 92168 | tf_op jit(solution)/shard_map/ppermute | solution.py:537
  10.9 2.5 %hold_caches.1 = (bf16[6,256,128]{2,1,0:T(8,128)(2,1)S(1)}, bf16[6,256,128]{2,1,0:T(8,128)(2,1)S(1)}, f32[6,2,256]{2,1,0:T(2,128)S(1)}, bf16[2048,1024]{1,0:T(8,128)(2,1)S(1)}, bf16[6,1024]{1,0:T(8,128)(2,1)S(1)}) custom-call(bf16[120,128]{1,0:T(8,128)(2,1)S(1)} %project.1.refs_0_, bf16[6,256,128]{2,1,0:T(8,128)(2,1)} %refs_1_.1, ...), custom_call_target="tpu_custom_call" | custom-call | flops 60063744 | bytes 5005312 | tf_op jit(solution)/shard_map/hold_caches/pallas_call | solution.py:187
  13.4 0.0 collective-permute-done.2.refs_3_
  13.4 1.6 %collective-permute-done.1.refs_2_ = bf16[120,128]{1,0:T(8,128)(2,1)S(1)} collective-permute-done((bf16[120,128]{1,0:T(8,128)(2,1)S(1)}, bf16[120,128]{1,0:T(8,128)(2,1)S(1)}, u32[]{:S(2)}, u32[]{:S(2)}) %collective-permute-start.1) | collective-permute-done | bytes 30752 | tf_op jit(solution)/shard_map/ppermute | solution.py:537
  15.0 0.0 collective-permute-done.refs_1_
  15.0 0.0 copy-done.2
  15.1 0.0 copy-done.1
  15.1 2.5 %attend.1._.refs_0_ = bf16[112,128]{1,0:T(8,128)(2,1)S(1)} custom-call(s32[6]{0:T(128)S(1)} %copy-done.1, f32[2]{0:T(128)S(1)} %copy-done.2, bf16[6,256,128]{2,1,0:T(8,128)(2,1)S(1)} %get-tuple-element.14.keys, bf16[6,256,128]{2,1,0:T(8,128)(2,1)S(1)} %get-tuple-element.15.values, f32[6,2,256]{2,1,0:T(2,128)S(1)} %get-tuple-element.16.gates, ...), custom_call_target="tpu_custom_call" | custom-call | flops 786432 | bytes 65536 | tf_op jit(solution)/shard_map/attend/pallas_call | solution.py:187
  17.5 2.2 %collective-permute-start.5 = (bf16[112,128]{1,0:T(8,128)(2,1)S(1)}, bf16[112,128]{1,0:T(8,128)(2,1)S(1)}, u32[]{:S(2)}, u32[]{:S(2)}) collective-permute-start(bf16[112,128]{1,0:T(8,128)(2,1)S(1)} %attend.1._.refs_0_), channel_id=1, source_target_pairs={{0,6},{2,4},{4,2},{6,0},{1,7},{3,5},{5,3},{7,1},{8,14},{10,12},{12... | collective-permute-start | bytes 86024 | tf_op jit(solution)/shard_map/ppermute | solution.py:537
  19.7 0.0 collective-permute-start.4
  19.7 2.2 %collective-permute-start.3 = (bf16[112,128]{1,0:T(8,128)(2,1)S(1)}, bf16[112,128]{1,0:T(8,128)(2,1)S(1)}, u32[]{:S(2)}, u32[]{:S(2)}) collective-permute-start(bf16[112,128]{1,0:T(8,128)(2,1)S(1)} %attend.1._.refs_0_), channel_id=1, source_target_pairs={{0,2},{2,0},{4,6},{6,4},{1,3},{3,1},{5,7},{7,5},{8,10},{10,8},{12,... | collective-permute-start | bytes 86024 | tf_op jit(solution)/shard_map/ppermute | solution.py:537
  21.9 3.5 %hold_low.1._.up_low = bf16[2048,2048]{1,0:T(8,128)(2,1)S(1)} custom-call(bf16[112,128]{1,0:T(8,128)(2,1)S(1)} %attend.1._.refs_0_, bf16[4096,2048]{1,0:T(8,128)(2,1)} %source.3), custom_call_target="tpu_custom_call" | custom-call | flops 100663296 | bytes 8388608 | tf_op jit(solution)/shard_map/hold_low/pallas_call | solution.py:187
  25.4 0.0 collective-permute-done.5.refs_3_
  25.4 0.0 collective-permute-done.4.refs_2_
  25.4 0.0 collective-permute-done.3.refs_1_
  25.4 0.9 %output.1 = (bf16[6,1024]{1,0:T(8,128)(2,1)S(1)}, f32[6,1024]{1,0:T(8,128)S(1)}) custom-call(bf16[2048,1024]{1,0:T(8,128)(2,1)S(1)} %get-tuple-element.17.weight, bf16[6,1024]{1,0:T(8,128)(2,1)S(1)} %get-tuple-element.18.tokens, bf16[2048,2048]{1,0:T(8,128)(2,1)S(1)} %hold_low.1._.up_low, bf16[112,128]{1,0:T(8,128)(2,1)S(1)} %attend.1._.refs_0_, ...), custom_call_target="tpu_custom_call" | custom-call | flops 786432 | bytes 65536 | tf_op jit(solution)/shard_map/output/pallas_call | solution.py:187
  26.4 0.0 collective-permute-start.6
  26.4 1.2 %collective-permute-done.6 = bf16[6,1024]{1,0:T(8,128)(2,1)S(1)} collective-permute-done((bf16[6,1024]{1,0:T(8,128)(2,1)S(1)}, bf16[6,1024]{1,0:T(8,128)(2,1)S(1)}, u32[]{:S(2)}, u32[]{:S(2)}) %collective-permute-start.6) | collective-permute-done | bytes 12320 | tf_op jit(solution)/shard_map/ppermute | solution.py:537
  27.6 0.0 copy-start
  27.6 2.2 %collective-permute-start.9 = (bf16[6,1024]{1,0:T(8,128)(2,1)S(1)}, bf16[6,1024]{1,0:T(8,128)(2,1)S(1)}, u32[]{:S(2)}, u32[]{:S(2)}) collective-permute-start(bf16[6,1024]{1,0:T(8,128)(2,1)S(1)} %add_convert_fusion._.refs_0_), channel_id=1, source_target_pairs={{0,6},{2,4},{4,2},{6,0},{1,7},{3,5},{5,3},{7,1},{8,14},{10,12},{12... | collective-permute-start | bytes 36872 | tf_op jit(solution)/shard_map/ppermute | solution.py:537
  29.8 0.0 collective-permute-start.8
  29.8 2.2 %collective-permute-start.7 = (bf16[6,1024]{1,0:T(8,128)(2,1)S(1)}, bf16[6,1024]{1,0:T(8,128)(2,1)S(1)}, u32[]{:S(2)}, u32[]{:S(2)}) collective-permute-start(bf16[6,1024]{1,0:T(8,128)(2,1)S(1)} %add_convert_fusion._.refs_0_), channel_id=1, source_target_pairs={{0,2},{2,0},{4,6},{6,4},{1,3},{3,1},{5,7},{7,5},{8,10},{10,8},{12,... | collective-permute-start | bytes 36872 | tf_op jit(solution)/shard_map/ppermute | solution.py:537
  32.0 3.5 %hold_high.1.up_high = bf16[2048,2048]{1,0:T(8,128)(2,1)S(1)} custom-call(bf16[6,1024]{1,0:T(8,128)(2,1)S(1)} %add_convert_fusion._.refs_0_, bf16[4096,2048]{1,0:T(8,128)(2,1)} %source.3), custom_call_target="tpu_custom_call" | custom-call | flops 100663296 | bytes 8388608 | tf_op jit(solution)/shard_map/hold_high/pallas_call | solution.py:187
  35.5 0.0 collective-permute-done.9.refs_3_
  35.6 0.0 collective-permute-done.8.refs_2_
  35.6 0.0 collective-permute-done.7.refs_1_
  35.6 0.0 copy-done
  35.6 6.6 %mixer.1 = (f32[4,6,512]{2,1,0:T(8,128)S(1)}, bf16[4,6,512]{2,1,0:T(8,128)(2,1)S(1)}) custom-call(f32[4,1,1024]{2,1,0:T(1,128)S(1)} %bitcast.18, bf16[2048,2048]{1,0:T(8,128)(2,1)S(1)} %hold_low.1._.up_low, bf16[2048,2048]{1,0:T(8,128)(2,1)S(1)} %hold_high.1.up_high, bf16[2048,4096]{1,0:T(8,128)(2,1)} %down_hbm.1, ...), custom_call_target="tpu_custom_call" | custom-call | flops 201326592 | bytes 16777216 | tf_op jit(solution)/shard_map/mixer/pallas_call | solution.py:187
  42.2 0.1 collective-permute-start.10
  42.2 1.2 %collective-permute-done.10 = bf16[4,6,512]{2,1,0:T(8,128)(2,1)S(1)} collective-permute-done((bf16[4,6,512]{2,1,0:T(8,128)(2,1)S(1)}, bf16[4,6,512]{2,1,0:T(8,128)(2,1)S(1)}, u32[]{:S(2)}, u32[]{:S(2)}) %collective-permute-start.10) | collective-permute-done | bytes 24608 | tf_op jit(solution)/shard_map/ppermute | solution.py:537
  43.5 0.3 collective-permute-start.11
  43.7 2.1 %collective-permute-start.13 = (bf16[6,512]{1,0:T(8,128)(2,1)S(1)}, bf16[6,512]{1,0:T(8,128)(2,1)S(1)}, u32[]{:S(2)}, u32[]{:S(2)}) collective-permute-start(bf16[6,512]{1,0:T(8,128)(2,1)S(1)} %get-tuple-element.26), channel_id=1, source_target_pairs={{0,6},{2,4},{4,2},{6,0},{1,7},{3,5},{5,3},{7,1},{8,14},{10,12},{12... | collective-permute-start | bytes 18440 | tf_op jit(solution)/shard_map/ppermute | solution.py:537
  45.9 1.2 %collective-permute-start.12 = (bf16[6,512]{1,0:T(8,128)(2,1)S(1)}, bf16[6,512]{1,0:T(8,128)(2,1)S(1)}, u32[]{:S(2)}, u32[]{:S(2)}) collective-permute-start(bf16[6,512]{1,0:T(8,128)(2,1)S(1)} %get-tuple-element.27), channel_id=1, source_target_pairs={{0,4},{2,6},{4,0},{6,2},{1,5},{3,7},{5,1},{7,3},{8,12},{10,14},{12... | collective-permute-start | bytes 18440 | tf_op jit(solution)/shard_map/ppermute | solution.py:537
  47.0 0.2 collective-permute-done.11
  47.2 2.0 %collective-permute-done.13 = bf16[6,512]{1,0:T(8,128)(2,1)S(1)} collective-permute-done((bf16[6,512]{1,0:T(8,128)(2,1)S(1)}, bf16[6,512]{1,0:T(8,128)(2,1)S(1)}, u32[]{:S(2)}, u32[]{:S(2)}) %collective-permute-start.13) | collective-permute-done | bytes 6176 | tf_op jit(solution)/shard_map/ppermute | solution.py:537
  49.2 1.2 %collective-permute-done.12 = bf16[6,512]{1,0:T(8,128)(2,1)S(1)} collective-permute-done((bf16[6,512]{1,0:T(8,128)(2,1)S(1)}, bf16[6,512]{1,0:T(8,128)(2,1)S(1)}, u32[]{:S(2)}, u32[]{:S(2)}) %collective-permute-start.12) | collective-permute-done | bytes 6176 | tf_op jit(solution)/shard_map/ppermute | solution.py:537
  50.4 0.6 %fusion.3 = bf16[6,512]{1,0:T(8,128)(2,1)} fusion(f32[4,6,512]{2,1,0:T(8,128)S(1)} %get-tuple-element.24, bf16[6,512]{1,0:T(8,128)(2,1)S(1)} %collective-permute-done.13, bf16[6,512]{1,0:T(8,128)(2,1)S(1)} %collective-permute-done.12, bf16[6,512]{1,0:T(8,128)(2,1)S(1)} %collective-permute-done.11), kind=kLoop, calls=%fused_computation.6 | loop fusion | flops 21504 | bytes 36864 | tf_op jit(solution)/shard_map/convert_element_type | solution.py:659
  (3 shorter events, 0.0 us)
Async XLA Ops:
  0.0 15.1 %copy-start.2 = (f32[2]{0:T(128)S(1)}, f32[2]{0:T(128)}, u32[]{:S(2)}) copy-start(f32[2]{0:T(128)} %offset.1) | copy-start | bytes 28
  0.0 15.1 %copy-start.1 = (s32[6]{0:T(128)S(1)}, s32[6]{0:T(128)}, u32[]{:S(2)}) copy-start(s32[6]{0:T(128)} %lengths.1) | copy-start | bytes 76
  5.1 8.3 %collective-permute-start.2 = (bf16[120,128]{1,0:T(8,128)(2,1)S(1)}, bf16[120,128]{1,0:T(8,128)(2,1)S(1)}, u32[]{:S(2)}, u32[]{:S(2)}) collective-permute-start(bf16[120,128]{1,0:T(8,128)(2,1)S(1)} %project.1.refs_0_), channel_id=1, source_target_pairs={{0,6},{2,4},{4,2},{6,0},{1,7},{3,5},{5,3},{7,1},{8,14},{10,12},{12... | collective-permute-start | bytes 92168 | tf_op jit(solution)/shard_map/ppermute | solution.py:537
  10.3 4.8 %collective-permute-start.1 = (bf16[120,128]{1,0:T(8,128)(2,1)S(1)}, bf16[120,128]{1,0:T(8,128)(2,1)S(1)}, u32[]{:S(2)}, u32[]{:S(2)}) collective-permute-start(bf16[120,128]{1,0:T(8,128)(2,1)S(1)} %project.1.refs_0_), channel_id=1, source_target_pairs={{0,4},{2,6},{4,0},{6,2},{1,5},{3,7},{5,1},{7,3},{8,12},{10,14},{12... | collective-permute-start | bytes 92168 | tf_op jit(solution)/shard_map/ppermute | solution.py:537
  10.3 4.8 %collective-permute-start = (bf16[120,128]{1,0:T(8,128)(2,1)S(1)}, bf16[120,128]{1,0:T(8,128)(2,1)S(1)}, u32[]{:S(2)}, u32[]{:S(2)}) collective-permute-start(bf16[120,128]{1,0:T(8,128)(2,1)S(1)} %project.1.refs_0_), channel_id=1, source_target_pairs={{0,2},{2,0},{4,6},{6,4},{1,3},{3,1},{5,7},{7,5},{8,10},{10,8},{12,... | collective-permute-start | bytes 92168 | tf_op jit(solution)/shard_map/ppermute | solution.py:537
  17.5 7.9 %collective-permute-start.5 = (bf16[112,128]{1,0:T(8,128)(2,1)S(1)}, bf16[112,128]{1,0:T(8,128)(2,1)S(1)}, u32[]{:S(2)}, u32[]{:S(2)}) collective-permute-start(bf16[112,128]{1,0:T(8,128)(2,1)S(1)} %attend.1._.refs_0_), channel_id=1, source_target_pairs={{0,6},{2,4},{4,2},{6,0},{1,7},{3,5},{5,3},{7,1},{8,14},{10,12},{12... | collective-permute-start | bytes 86024 | tf_op jit(solution)/shard_map/ppermute | solution.py:537
  19.7 5.8 %collective-permute-start.4 = (bf16[112,128]{1,0:T(8,128)(2,1)S(1)}, bf16[112,128]{1,0:T(8,128)(2,1)S(1)}, u32[]{:S(2)}, u32[]{:S(2)}) collective-permute-start(bf16[112,128]{1,0:T(8,128)(2,1)S(1)} %attend.1._.refs_0_), channel_id=1, source_target_pairs={{0,4},{2,6},{4,0},{6,2},{1,5},{3,7},{5,1},{7,3},{8,12},{10,14},{12... | collective-permute-start | bytes 86024 | tf_op jit(solution)/shard_map/ppermute | solution.py:537
  19.7 5.8 %collective-permute-start.3 = (bf16[112,128]{1,0:T(8,128)(2,1)S(1)}, bf16[112,128]{1,0:T(8,128)(2,1)S(1)}, u32[]{:S(2)}, u32[]{:S(2)}) collective-permute-start(bf16[112,128]{1,0:T(8,128)(2,1)S(1)} %attend.1._.refs_0_), channel_id=1, source_target_pairs={{0,2},{2,0},{4,6},{6,4},{1,3},{3,1},{5,7},{7,5},{8,10},{10,8},{12,... | collective-permute-start | bytes 86024 | tf_op jit(solution)/shard_map/ppermute | solution.py:537
  26.4 1.2 %collective-permute-start.6 = (bf16[6,1024]{1,0:T(8,128)(2,1)S(1)}, bf16[6,1024]{1,0:T(8,128)(2,1)S(1)}, u32[]{:S(2)}, u32[]{:S(2)}) collective-permute-start(bf16[6,1024]{1,0:T(8,128)(2,1)S(1)} %get-tuple-element.20), channel_id=1, source_target_pairs={{0,1},{1,0},{2,3},{3,2},{4,5},{5,4},{6,7},{7,6},{8,9},{9,8},{10,11... | collective-permute-start | bytes 36872 | tf_op jit(solution)/shard_map/ppermute | solution.py:537
  27.6 8.0 %copy-start = (f32[4096]{0:T(1024)S(1)}, f32[4096]{0:T(1024)}, u32[]{:S(2)}) copy-start(f32[4096]{0:T(1024)} %param.27) | copy-start | bytes 49156
  27.6 8.0 %collective-permute-start.9 = (bf16[6,1024]{1,0:T(8,128)(2,1)S(1)}, bf16[6,1024]{1,0:T(8,128)(2,1)S(1)}, u32[]{:S(2)}, u32[]{:S(2)}) collective-permute-start(bf16[6,1024]{1,0:T(8,128)(2,1)S(1)} %add_convert_fusion._.refs_0_), channel_id=1, source_target_pairs={{0,6},{2,4},{4,2},{6,0},{1,7},{3,5},{5,3},{7,1},{8,14},{10,12},{12... | collective-permute-start | bytes 36872 | tf_op jit(solution)/shard_map/ppermute | solution.py:537
  29.8 5.8 %collective-permute-start.8 = (bf16[6,1024]{1,0:T(8,128)(2,1)S(1)}, bf16[6,1024]{1,0:T(8,128)(2,1)S(1)}, u32[]{:S(2)}, u32[]{:S(2)}) collective-permute-start(bf16[6,1024]{1,0:T(8,128)(2,1)S(1)} %add_convert_fusion._.refs_0_), channel_id=1, source_target_pairs={{0,4},{2,6},{4,0},{6,2},{1,5},{3,7},{5,1},{7,3},{8,12},{10,14},{12... | collective-permute-start | bytes 36872 | tf_op jit(solution)/shard_map/ppermute | solution.py:537
  29.8 5.8 %collective-permute-start.7 = (bf16[6,1024]{1,0:T(8,128)(2,1)S(1)}, bf16[6,1024]{1,0:T(8,128)(2,1)S(1)}, u32[]{:S(2)}, u32[]{:S(2)}) collective-permute-start(bf16[6,1024]{1,0:T(8,128)(2,1)S(1)} %add_convert_fusion._.refs_0_), channel_id=1, source_target_pairs={{0,2},{2,0},{4,6},{6,4},{1,3},{3,1},{5,7},{7,5},{8,10},{10,8},{12,... | collective-permute-start | bytes 36872 | tf_op jit(solution)/shard_map/ppermute | solution.py:537
  42.2 1.3 %collective-permute-start.10 = (bf16[4,6,512]{2,1,0:T(8,128)(2,1)S(1)}, bf16[4,6,512]{2,1,0:T(8,128)(2,1)S(1)}, u32[]{:S(2)}, u32[]{:S(2)}) collective-permute-start(bf16[4,6,512]{2,1,0:T(8,128)(2,1)S(1)} %get-tuple-element.22), channel_id=1, source_target_pairs={{0,1},{1,0},{2,3},{3,2},{4,5},{5,4},{6,7},{7,6},{8,9},{9,8},{10,11... | collective-permute-start | bytes 73736 | tf_op jit(solution)/shard_map/ppermute | solution.py:537
  43.5 3.7 %collective-permute-start.11 = (bf16[6,512]{1,0:T(8,128)(2,1)S(1)}, bf16[6,512]{1,0:T(8,128)(2,1)S(1)}, u32[]{:S(2)}, u32[]{:S(2)}) collective-permute-start(bf16[6,512]{1,0:T(8,128)(2,1)S(1)} %get-tuple-element.25), channel_id=1, source_target_pairs={{0,2},{2,0},{4,6},{6,4},{1,3},{3,1},{5,7},{7,5},{8,10},{10,8},{12,... | collective-permute-start | bytes 18440 | tf_op jit(solution)/shard_map/ppermute | solution.py:537
  43.7 5.4 %collective-permute-start.13 = (bf16[6,512]{1,0:T(8,128)(2,1)S(1)}, bf16[6,512]{1,0:T(8,128)(2,1)S(1)}, u32[]{:S(2)}, u32[]{:S(2)}) collective-permute-start(bf16[6,512]{1,0:T(8,128)(2,1)S(1)} %get-tuple-element.26), channel_id=1, source_target_pairs={{0,6},{2,4},{4,2},{6,0},{1,7},{3,5},{5,3},{7,1},{8,14},{10,12},{12... | collective-permute-start | bytes 18440 | tf_op jit(solution)/shard_map/ppermute | solution.py:537
  45.9 4.5 %collective-permute-start.12 = (bf16[6,512]{1,0:T(8,128)(2,1)S(1)}, bf16[6,512]{1,0:T(8,128)(2,1)S(1)}, u32[]{:S(2)}, u32[]{:S(2)}) collective-permute-start(bf16[6,512]{1,0:T(8,128)(2,1)S(1)} %get-tuple-element.27), channel_id=1, source_target_pairs={{0,4},{2,6},{4,0},{6,2},{1,5},{3,7},{5,1},{7,3},{8,12},{10,14},{12... | collective-permute-start | bytes 18440 | tf_op jit(solution)/shard_map/ppermute | solution.py:537

commit v2 on v1

--- a/solution.py
+++ b/solution.py
@@ -182,7 +182,15 @@
 anywhere = pl.BlockSpec(memory_space=pl.ANY)
 
 
-def call(kernel, outs, in_specs, args, scratch=(), megabytes=8, weight_bytes=0, name=None):
+HOLD_WORK = 10**10
+PROJECT_WORK = 10**8
+ATTEND_WORK = 10**10
+MERGE_WORK = 10**10
+NORM_WORK = 10**8
+SPREAD_WORK = 10**8
+
+
+def call(kernel, outs, in_specs, args, scratch=(), megabytes=8, work=1 << 20, name=None):
     many = isinstance(outs, (list, tuple))
     return pl.pallas_call(
         kernel,
@@ -192,8 +200,8 @@
         scratch_shapes=list(scratch),
         compiler_params=pltpu.CompilerParams(vmem_limit_bytes=megabytes * 1024 * 1024),
         cost_estimate=pl.CostEstimate(
-            flops=12 * max(weight_bytes, 1 << 16),
-            bytes_accessed=max(weight_bytes, 1 << 16),
+            flops=work,
+            bytes_accessed=1 << 16,
             transcendentals=0,
         ),
         name=name,
@@ -237,7 +245,7 @@
     copies = [
         pltpu.make_async_copy(tokens_hbm, tokens, sems.at[0]),
         pltpu.make_async_copy(gain_hbm, gain, sems.at[1]),
-        pltpu.make_async_copy(forget_hbm.at[pl.ds(start, feats), :], forget, sems.at[2]),
+        pltpu.make_async_copy(forget_hbm.at[:, pl.ds(start, feats)], forget, sems.at[2]),
         pltpu.make_async_copy(key_hbm, key, sems.at[3]),
         pltpu.make_async_copy(value_hbm, value, sems.at[4]),
     ]
@@ -269,7 +277,9 @@
         copy.wait()
     key_part = jnp.dot(scaled, key[...], preferred_element_type=f32)
     value_part = jnp.dot(scaled, value[...], preferred_element_type=f32)
-    forget_part = jnp.dot(scaled, forget[...], preferred_element_type=f32)
+    forget_part = lax.dot_general(
+        scaled, forget[...], (((1,), (1,)), ((), ())), preferred_element_type=f32
+    )
     heads = forget_part.shape[1]
     lane = lane_index(rows)
     extra = jnp.where(lane == heads, squares, 0.0)
@@ -303,7 +313,6 @@
 
 def hold(after, arrays, name):
     outs = [pltpu.VMEM(a.shape, a.dtype) for a in arrays]
-    size = sum(a.size * a.dtype.itemsize for a in arrays)
     return call(
         functools.partial(hold_kernel, len(arrays)),
         outs,
@@ -311,37 +320,7 @@
         [after] + [pinned(a, HBM) for a in arrays],
         scratch=[pltpu.SemaphoreType.DMA((len(arrays),))],
         megabytes=1,
-        weight_bytes=size,
-        name=name,
-    )
-
-
-def hold_rows_kernel(first, count, pieces, _, source, target, sems):
-    depth = count // pieces
-    copies = [
-        pltpu.make_async_copy(
-            source.at[pl.ds(first + i * depth, depth), :],
-            target.at[pl.ds(i * depth, depth), :],
-            sems.at[i],
-        )
-        for i in range(pieces)
-    ]
-    for copy in copies:
-        copy.start()
-    for copy in copies:
-        copy.wait()
-
-
-def hold_rows(after, array, first, count, name):
-    pieces = 4
-    return call(
-        functools.partial(hold_rows_kernel, first, count, pieces),
-        pltpu.VMEM((count, array.shape[1]), array.dtype),
-        [anywhere, in_hbm],
-        [after, pinned(array, HBM)],
-        scratch=[pltpu.SemaphoreType.DMA((pieces,))],
-        megabytes=1,
-        weight_bytes=count * array.shape[1] * array.dtype.itemsize,
+        work=HOLD_WORK,
         name=name,
     )
 
@@ -441,9 +420,9 @@
     sent_ref[rows * tiles :, :] = stats.astype(bf16)
 
 
-def output_kernel(peers, rows, weight, tokens, _, *refs):
+def merge_kernel(peers, rows, *refs):
     parts = refs[:peers]
-    partial_ref, kept_ref, stage = refs[peers:]
+    attended_ref, stage = refs[peers:]
     tiles = parts[0].shape[0] // (rows + 1)
     quarter = LANES // 4
     tops, totals = [], []
@@ -468,31 +447,19 @@
             term = part[b * tiles : (b + 1) * tiles, :].astype(f32) * factor
             mixed = term if mixed is None else mixed + term
         stage[b * tiles : (b + 1) * tiles, :] = mixed
-    attended = jnp.concatenate(
-        [stage[pl.ds(c, rows, stride=tiles), :] for c in range(tiles)], axis=1
-    ).astype(bf16)
-    partial = jnp.dot(attended, weight[...], preferred_element_type=f32).astype(bf16)
-    partial_ref[...] = partial
-    kept_ref[...] = tokens[...].astype(f32) + partial.astype(f32)
-
-
-def mixer_kernel(
-    peers, gain, up_low, up_high, down_hbm, *refs
-):
+    for c in range(tiles):
+        attended_ref[:, c * LANES : (c + 1) * LANES] = stage[
+            pl.ds(c, rows, stride=tiles), :
+        ].astype(bf16)
+
+
+def norm_kernel(peers, gain, *refs):
     mids = refs[:peers]
-    kept_ref, sent_ref, down, normed, spread, sems = refs[peers:]
-    rows, width = mids[0].shape
-    chunks, depth = down.shape[:2]
+    normed_ref, share_ref, ordered = refs[peers:]
+    width = mids[0].shape[1]
+    cols = share_ref.shape[1]
     kv_place = lax.axis_index("kv")
     tp_place = lax.axis_index("tp")
-    streams = [
-        pltpu.make_async_copy(
-            down_hbm.at[pl.ds(i * depth, depth), :], down.at[i], sems.at[i]
-        )
-        for i in range(chunks)
-    ]
-    for copy in streams:
-        copy.start()
     wides = [m[...].astype(f32) for m in mids]
     squares = functools.reduce(
         jnp.add, [jnp.sum(w * w, axis=1, keepdims=True) for w in wides]
@@ -500,37 +467,23 @@
     scale = lax.rsqrt(squares / D + epsilon)
     for k in range(peers):
         source = kv_place ^ k
-        normed[source] = wides[k] * gain[source] * scale
-    half = peers // 2
-    hidden = None
+        ordered[source] = wides[k] * gain[source] * scale
     for j in range(peers):
-        up = up_low if j < half else up_high
-        first = (j % half) * width
-        term = jnp.dot(
-            normed[j].astype(bf16), up[first : first + width, :], preferred_element_type=f32
-        )
-        hidden = term if hidden is None else hidden + term
-    hidden = jnp.square(jnp.maximum(hidden, 0.0)).astype(bf16)
-    total = None
-    for i in range(chunks):
-        streams[i].wait()
-        term = jnp.dot(
-            hidden[:, i * depth : (i + 1) * depth], down[i], preferred_element_type=f32
-        )
-        total = term if total is None else total + term
-    blocks = spread.shape[0]
-    cols = spread.shape[2]
+        normed_ref[:, j * width : (j + 1) * width] = ordered[j].astype(bf16)
+    share_ref[...] = jnp.where(tp_place == 0, wides[0][:, :cols], wides[0][:, cols:])
+
+
+def spread_kernel(peers, mixed, share, kept_ref, sent_ref, spread):
+    blocks, _, cols = spread.shape
+    kv_place = lax.axis_index("kv")
+    tp_place = lax.axis_index("tp")
     for q in range(blocks):
-        spread[q] = total[:, q * cols : (q + 1) * cols]
+        spread[q] = mixed[:, q * cols : (q + 1) * cols]
     for k in range(peers):
         target = 2 * (kv_place ^ k)
-        kept_ref[k] = spread[target + tp_place]
+        own = spread[target + tp_place]
+        kept_ref[k] = own + share[...] if k == 0 else own
         sent_ref[k] = spread[target + 1 - tp_place].astype(bf16)
-    for half_place in range(2):
-
-        @pl.when(tp_place == half_place)
-        def _():
-            kept_ref[0] += mids[0][:, half_place * cols : (half_place + 1) * cols].astype(f32)
 
 
 def swap(x, axis, k):
@@ -573,7 +526,7 @@
                 query_weight,
                 key_weight,
                 value_weight,
-                forget_weight,
+                forget_weight.T,
             )
         ],
         scratch=[
@@ -582,17 +535,17 @@
             pltpu.VMEM((chunks, depth, query_weight.shape[1]), bf16),
             pltpu.VMEM(key_weight.shape, bf16),
             pltpu.VMEM(value_weight.shape, bf16),
-            pltpu.VMEM((feats, forget_weight.shape[1]), bf16),
+            pltpu.VMEM((forget_weight.shape[1], feats), bf16),
             pltpu.VMEM((part_rows, LANES), f32),
             pltpu.SemaphoreType.DMA((5 + chunks,)),
         ],
         megabytes=12,
-        weight_bytes=query_weight.size * 2,
+        work=PROJECT_WORK,
         name="project",
     )
     parts = [part] + [swap(part, "kv", k) for k in others]
-    keys_held, values_held, gates_held, out_held, tokens_held = hold(
-        part, [cache_keys, cache_values, gate_sum, out_weight, tokens], "hold_caches"
+    keys_held, values_held, gates_held = hold(
+        part, [cache_keys, cache_values, gate_sum], "hold_caches"
     )
     sent = call(
         functools.partial(attend_kernel, peers, rows),
@@ -603,53 +556,58 @@
         + parts,
         scratch=[pltpu.VMEM((part_rows, LANES), f32)],
         megabytes=6,
+        work=ATTEND_WORK,
         name="attend",
     )
     sents = [sent] + [swap(sent, "kv", k) for k in others]
-    total_rows = up_weight.shape[0]
-    up_low = hold_rows(sent, up_weight, 0, total_rows // 2, "hold_low")
-    partial, kept = call(
-        functools.partial(output_kernel, peers, rows),
-        [
-            jax.ShapeDtypeStruct((rows, out_weight.shape[1]), bf16),
-            jax.ShapeDtypeStruct((rows, out_weight.shape[1]), f32),
-        ],
-        [in_vmem] * 2 + [anywhere] + [in_vmem] * peers,
-        [pinned(out_held, VMEM), pinned(tokens_held, VMEM), pinned(up_low, VMEM)] + sents,
+    attended = call(
+        functools.partial(merge_kernel, peers, rows),
+        jax.ShapeDtypeStruct((rows, tiles * LANES), bf16),
+        [in_vmem] * peers,
+        sents,
         scratch=[pltpu.VMEM((rows * tiles, LANES), f32)],
         megabytes=6,
-        name="output",
-    )
-    mid = (kept + swap(partial, "tp", 1).astype(f32)).astype(bf16)
+        work=MERGE_WORK,
+        name="merge",
+    )
+    partial = jnp.dot(attended, out_weight, preferred_element_type=f32).astype(bf16)
+    mid = (
+        tokens.astype(f32) + partial.astype(f32) + swap(partial, "tp", 1).astype(f32)
+    ).astype(bf16)
     mids = [mid] + [swap(mid, "kv", k) for k in others]
-    up_high = hold_rows(mid, up_weight, total_rows // 2, total_rows // 2, "hold_high")
-    hidden_rows, model = down_weight.shape
-    pieces = 8
+    model = down_weight.shape[1]
     blocks = 2 * peers
     cols = model // blocks
+    normed, share = call(
+        functools.partial(norm_kernel, peers),
+        [
+            jax.ShapeDtypeStruct((rows, model), bf16),
+            jax.ShapeDtypeStruct((rows, cols), f32),
+        ],
+        [in_vmem] * (1 + peers),
+        [mlp_gain.reshape(peers, 1, model // peers)] + mids,
+        scratch=[pltpu.VMEM((peers, rows, model // peers), f32)],
+        megabytes=4,
+        work=NORM_WORK,
+        name="norm",
+    )
+    hidden = jnp.square(
+        jax.nn.relu(jnp.dot(normed, up_weight, preferred_element_type=f32))
+    ).astype(bf16)
+    hidden = lax.optimization_barrier(hidden)
+    mixed = jnp.dot(hidden, down_weight, preferred_element_type=f32)
     kept, crossing = call(
-        functools.partial(mixer_kernel, peers),
+        functools.partial(spread_kernel, peers),
         [
             jax.ShapeDtypeStruct((peers, rows, cols), f32),
             jax.ShapeDtypeStruct((peers, rows, cols), bf16),
         ],
-        [in_vmem] * 3 + [in_hbm] + [in_vmem] * peers,
-        [
-            mlp_gain.reshape(peers, 1, model // peers),
-            pinned(up_low, VMEM),
-            pinned(up_high, VMEM),
-            pinned(down_weight, HBM),
-        ]
-        + mids,
-        scratch=[
-            pltpu.VMEM((pieces, hidden_rows // pieces, model), bf16),
-            pltpu.VMEM((peers, rows, model // peers), f32),
-            pltpu.VMEM((blocks, rows, cols), f32),
-            pltpu.SemaphoreType.DMA((pieces,)),
-        ],
-        megabytes=24,
-        weight_bytes=down_weight.size * 2,
-        name="mixer",
+        [in_vmem] * 2,
+        [mixed, share],
+        scratch=[pltpu.VMEM((blocks, rows, cols), f32)],
+        megabytes=4,
+        work=SPREAD_WORK,
+        name="spread",
     )
     paired = kept + swap(crossing, "tp", 1).astype(f32)
     shares = [swap(paired[k].astype(bf16), "kv", k) for k in others]

time: 51.3 us -> 46.3 us (0.903)
  Pallas kernels: 22.4 us -> 6.97 us
  waiting for transfers between devices: 7.43 us -> 14.7 us
  matrix products: 0 us -> 5.19 us
  local copies, waits for them, and re-layouts: 2.2 us -> 0.08 us
    pallas_call x7 -> x6, Pallas kernels: 22.4 us -> 6.97 us  [call(): pl.pallas_call(kernel, out_shape=outs, in_specs=in_specs, out_specs=[in_v...]
    ppermute x14, waiting for transfers between devices: 7.43 us -> 14.7 us  [swap(): lax.ppermute(x, axis, [(i, i ^ k) for i in range(lax.axis_size(axis))])]
    dot_general x0 -> x3, matrix products: none -> 5.19 us  [the longest x1 2.27 us: shards_direct(): jnp.dot(normed, up_weight, preferred_element_type=f32)]
    unnamed x7 -> x26, local copies, waits for them, and re-layouts: 2.2 us -> 0.07 us
  transfers between devices with their start and end apart: 14 -> 14, of which waited for: 6 -> 12; matrix products, arithmetic and copies ran while one was open for 0% -> 0% of each run, Pallas kernels for 19% -> 2%
where the time goes in v2:
time: 46.3 us; the launch traced here: 46.1 us
  starting transfers between devices  18.3 us (40%)
  waiting for transfers between devices  14.7 us (32%)
  Pallas kernels  6.97 us (15%)
  matrix products  5.19 us (11%)
  other arithmetic  0.63 us (1%)
    ppermute x14, starting transfers between devices, swap(): lax.ppermute(x, axis, [(i, i ^ k) for i in range(lax.axis_size(axis))])  18.3 us
    ppermute x14, waiting for transfers between devices, swap(): lax.ppermute(x, axis, [(i, i ^ k) for i in range(lax.axis_size(axis))])  14.7 us
    pallas_call x6, Pallas kernels, call(): pl.pallas_call(kernel, out_shape=outs, in_specs=in_specs, out_specs=[in_v...  6.97 us
    dot_general x1, matrix products, shards_direct(): jnp.dot(normed, up_weight, preferred_element_type=f32)  2.27 us
    dot_general x1, matrix products, shards_direct(): mixed = jnp.dot(hidden, down_weight, preferred_element_type=f32)  2.27 us
  transfers between devices with their start and end apart: 14, of which 12 were waited for; matrix products, arithmetic and copies ran while one was open for 0% of the time, Pallas kernels for 2%

profile of v2, /device:TPU:0, one launch (start us, length us, event | category | flops | bytes accessed | tf_op | source)
XLA Modules:
  0.0 46.1 jit_solution(17348186198786550345)
XLA Ops:
  0.0 2.9 %project.1.refs_0_ = bf16[120,128]{1,0:T(8,128)(2,1)S(1)} custom-call(bf16[6,1024]{1,0:T(8,128)(2,1)} %tokens_hbm.1, f32[1,1024]{1,0:T(1,128)} %bitcast.31, bf16[1024,2048]{1,0:T(8,128)(2,1)} %query_hbm.1, bf16[1024,128]{1,0:T(8,128)(2,1)} %key_hbm.1, bf16[1024,128]{1,0:T(8,128)(2,1)} %value_hbm.1, bf16[4,4096]{1,0:T(4,128)(2,1)} %bitcast.30), custom_call_target="tpu_custom_call" | custom-call | flops 100000000 | bytes 65536 | tf_op jit(solution)/shard_map/project/pallas_call | solution.py:195
  2.9 0.0 copy-start.1
  2.9 0.0 copy-start.2
  2.9 5.1 %collective-permute-start.2 = (bf16[120,128]{1,0:T(8,128)(2,1)S(1)}, bf16[120,128]{1,0:T(8,128)(2,1)S(1)}, u32[]{:S(2)}, u32[]{:S(2)}) collective-permute-start(bf16[120,128]{1,0:T(8,128)(2,1)S(1)} %project.1.refs_0_), channel_id=1, source_target_pairs={{0,6},{2,4},{4,2},{6,0},{1,7},{3,5},{5,3},{7,1},{8,14},{10,12},{12... | collective-permute-start | bytes 92168 | tf_op jit(solution)/shard_map/ppermute | solution.py:490
  8.1 0.0 collective-permute-start.1
  8.1 0.6 %collective-permute-start = (bf16[120,128]{1,0:T(8,128)(2,1)S(1)}, bf16[120,128]{1,0:T(8,128)(2,1)S(1)}, u32[]{:S(2)}, u32[]{:S(2)}) collective-permute-start(bf16[120,128]{1,0:T(8,128)(2,1)S(1)} %project.1.refs_0_), channel_id=1, source_target_pairs={{0,2},{2,0},{4,6},{6,4},{1,3},{3,1},{5,7},{7,5},{8,10},{10,8},{12,... | collective-permute-start | bytes 92168 | tf_op jit(solution)/shard_map/ppermute | solution.py:490
  8.7 1.1 %hold_caches.1 = (bf16[6,256,128]{2,1,0:T(8,128)(2,1)S(1)}, bf16[6,256,128]{2,1,0:T(8,128)(2,1)S(1)}, f32[6,2,256]{2,1,0:T(2,128)S(1)}) custom-call(bf16[120,128]{1,0:T(8,128)(2,1)S(1)} %project.1.refs_0_, bf16[6,256,128]{2,1,0:T(8,128)(2,1)} %refs_1_.1, bf16[6,256,128]{2,1,0:T(8,128)(2,1)} %refs_2_.1, f32[6,2,256]{2,1,0:T(2,128)} %refs_3_.1), custom_call_target="tpu_custom_call" | custom-call | flops 10000000000 | bytes 65536 | tf_op jit(solution)/shard_map/hold_caches/pallas_call | solution.py:195
  9.9 0.1 collective-permute-done.2.refs_3_
  9.9 2.9 %collective-permute-done.1.refs_2_ = bf16[120,128]{1,0:T(8,128)(2,1)S(1)} collective-permute-done((bf16[120,128]{1,0:T(8,128)(2,1)S(1)}, bf16[120,128]{1,0:T(8,128)(2,1)S(1)}, u32[]{:S(2)}, u32[]{:S(2)}) %collective-permute-start.1) | collective-permute-done | bytes 30752 | tf_op jit(solution)/shard_map/ppermute | solution.py:490
  12.9 0.0 collective-permute-done.refs_1_
  12.9 0.0 copy-done.1
  12.9 0.0 copy-done.2
  12.9 0.0 slice-start
  12.9 0.0 slice-start.1
  12.9 2.4 %attend.1.refs_0_ = bf16[112,128]{1,0:T(8,128)(2,1)S(1)} custom-call(s32[6]{0:T(128)S(1)} %copy-done.1, f32[2]{0:T(128)S(1)} %copy-done.2, bf16[6,256,128]{2,1,0:T(8,128)(2,1)S(1)} %get-tuple-element.12.keys, bf16[6,256,128]{2,1,0:T(8,128)(2,1)S(1)} %get-tuple-element.13.values, f32[6,2,256]{2,1,0:T(2,128)S(1)} %get-tuple-element.14.gates, ...), custom_call_target="tpu_custom_call" | custom-call | flops 10000000000 | bytes 65536 | tf_op jit(solution)/shard_map/attend/pallas_call | solution.py:195
  15.3 0.0 copy-start
  15.4 0.0 slice-start.2
  15.4 0.0 slice-start.3
  15.4 1.5 %collective-permute-start.5 = (bf16[112,128]{1,0:T(8,128)(2,1)S(1)}, bf16[112,128]{1,0:T(8,128)(2,1)S(1)}, u32[]{:S(2)}, u32[]{:S(2)}) collective-permute-start(bf16[112,128]{1,0:T(8,128)(2,1)S(1)} %attend.1.refs_0_), channel_id=1, source_target_pairs={{0,6},{2,4},{4,2},{6,0},{1,7},{3,5},{5,3},{7,1},{8,14},{10,12},{12... | collective-permute-start | bytes 86024 | tf_op jit(solution)/shard_map/ppermute | solution.py:490
  16.9 0.6 %collective-permute-start.4 = (bf16[112,128]{1,0:T(8,128)(2,1)S(1)}, bf16[112,128]{1,0:T(8,128)(2,1)S(1)}, u32[]{:S(2)}, u32[]{:S(2)}) collective-permute-start(bf16[112,128]{1,0:T(8,128)(2,1)S(1)} %attend.1.refs_0_), channel_id=1, source_target_pairs={{0,4},{2,6},{4,0},{6,2},{1,5},{3,7},{5,1},{7,3},{8,12},{10,14},{12... | collective-permute-start | bytes 86024 | tf_op jit(solution)/shard_map/ppermute | solution.py:490
  17.5 2.3 %collective-permute-start.3 = (bf16[112,128]{1,0:T(8,128)(2,1)S(1)}, bf16[112,128]{1,0:T(8,128)(2,1)S(1)}, u32[]{:S(2)}, u32[]{:S(2)}) collective-permute-start(bf16[112,128]{1,0:T(8,128)(2,1)S(1)} %attend.1.refs_0_), channel_id=1, source_target_pairs={{0,2},{2,0},{4,6},{6,4},{1,3},{3,1},{5,7},{7,5},{8,10},{10,8},{12,... | collective-permute-start | bytes 86024 | tf_op jit(solution)/shard_map/ppermute | solution.py:490
  19.8 1.3 %collective-permute-done.5.refs_3_ = bf16[112,128]{1,0:T(8,128)(2,1)S(1)} collective-permute-done((bf16[112,128]{1,0:T(8,128)(2,1)S(1)}, bf16[112,128]{1,0:T(8,128)(2,1)S(1)}, u32[]{:S(2)}, u32[]{:S(2)}) %collective-permute-start.5) | collective-permute-done | bytes 28704 | tf_op jit(solution)/shard_map/ppermute | solution.py:490
  21.1 0.6 %collective-permute-done.4.refs_2_ = bf16[112,128]{1,0:T(8,128)(2,1)S(1)} collective-permute-done((bf16[112,128]{1,0:T(8,128)(2,1)S(1)}, bf16[112,128]{1,0:T(8,128)(2,1)S(1)}, u32[]{:S(2)}, u32[]{:S(2)}) %collective-permute-start.4) | collective-permute-done | bytes 28704 | tf_op jit(solution)/shard_map/ppermute | solution.py:490
  21.7 0.3 collective-permute-done.3.refs_1_
  22.0 0.3 merge.1
  22.3 0.7 %convolution_convert_fusion = bf16[6,1024]{1,0:T(8,128)(2,1)S(1)} fusion(bf16[6,2048]{1,0:T(8,128)(2,1)S(1)} %merge.1, bf16[2048,1024]{1,0:T(8,128)(2,1)S(1)} %copy-done.3), kind=kOutput, calls=%fused_computation.3 | convolution fusion | flops 25171968 | bytes 4231168 | tf_op jit(solution)/shard_map/dot_general | solution.py:573
  23.0 0.0 collective-permute-start.6
  23.0 1.2 %collective-permute-done.6 = bf16[6,1024]{1,0:T(8,128)(2,1)S(1)} collective-permute-done((bf16[6,1024]{1,0:T(8,128)(2,1)S(1)}, bf16[6,1024]{1,0:T(8,128)(2,1)S(1)}, u32[]{:S(2)}, u32[]{:S(2)}) %collective-permute-start.6) | collective-permute-done | bytes 12320 | tf_op jit(solution)/shard_map/ppermute | solution.py:490
  24.2 2.4 %collective-permute-start.9 = (bf16[6,1024]{1,0:T(8,128)(2,1)S(1)}, bf16[6,1024]{1,0:T(8,128)(2,1)S(1)}, u32[]{:S(2)}, u32[]{:S(2)}) collective-permute-start(bf16[6,1024]{1,0:T(8,128)(2,1)S(1)} %add_convert_fusion.refs_0_), channel_id=1, source_target_pairs={{0,6},{2,4},{4,2},{6,0},{1,7},{3,5},{5,3},{7,1},{8,14},{10,12},{12... | collective-permute-start | bytes 36872 | tf_op jit(solution)/shard_map/ppermute | solution.py:490
  26.6 0.8 %collective-permute-start.8 = (bf16[6,1024]{1,0:T(8,128)(2,1)S(1)}, bf16[6,1024]{1,0:T(8,128)(2,1)S(1)}, u32[]{:S(2)}, u32[]{:S(2)}) collective-permute-start(bf16[6,1024]{1,0:T(8,128)(2,1)S(1)} %add_convert_fusion.refs_0_), channel_id=1, source_target_pairs={{0,4},{2,6},{4,0},{6,2},{1,5},{3,7},{5,1},{7,3},{8,12},{10,14},{12... | collective-permute-start | bytes 36872 | tf_op jit(solution)/shard_map/ppermute | solution.py:490
  27.4 1.2 %collective-permute-start.7 = (bf16[6,1024]{1,0:T(8,128)(2,1)S(1)}, bf16[6,1024]{1,0:T(8,128)(2,1)S(1)}, u32[]{:S(2)}, u32[]{:S(2)}) collective-permute-start(bf16[6,1024]{1,0:T(8,128)(2,1)S(1)} %add_convert_fusion.refs_0_), channel_id=1, source_target_pairs={{0,2},{2,0},{4,6},{6,4},{1,3},{3,1},{5,7},{7,5},{8,10},{10,8},{12,... | collective-permute-start | bytes 36872 | tf_op jit(solution)/shard_map/ppermute | solution.py:490
  28.6 1.2 %collective-permute-done.9.refs_3_ = bf16[6,1024]{1,0:T(8,128)(2,1)S(1)} collective-permute-done((bf16[6,1024]{1,0:T(8,128)(2,1)S(1)}, bf16[6,1024]{1,0:T(8,128)(2,1)S(1)}, u32[]{:S(2)}, u32[]{:S(2)}) %collective-permute-start.9) | collective-permute-done | bytes 12320 | tf_op jit(solution)/shard_map/ppermute | solution.py:490
  29.8 1.6 %collective-permute-done.8.refs_2_ = bf16[6,1024]{1,0:T(8,128)(2,1)S(1)} collective-permute-done((bf16[6,1024]{1,0:T(8,128)(2,1)S(1)}, bf16[6,1024]{1,0:T(8,128)(2,1)S(1)}, u32[]{:S(2)}, u32[]{:S(2)}) %collective-permute-start.8) | collective-permute-done | bytes 12320 | tf_op jit(solution)/shard_map/ppermute | solution.py:490
  31.4 0.0 collective-permute-done.7.refs_1_
  31.4 0.1 norm.1
  31.6 0.0 slice-start.7
  31.6 2.3 %fusion.1 = bf16[6,2048]{1,0:T(8,128)(2,1)S(1)} fusion(bf16[6,4096]{1,0:T(8,128)(2,1)S(1)} %get-tuple-element.15, bf16[4096,2048]{1,0:T(8,128)(2,1)S(1)} %bitcast.27), kind=kOutput, calls=%fused_computation.2 | convolution fusion | flops 100700160 | bytes 16850944 | tf_op jit(solution)/shard_map/dot_general | solution.py:595
  33.8 0.0 slice-done.5
  33.9 2.3 %fusion.7.mixed = f32[6,4096]{1,0:T(8,128)S(1)} fusion(bf16[6,2048]{1,0:T(8,128)(2,1)S(1)} %fusion.1, bf16[2048,4096]{1,0:T(8,128)(2,1)S(1)} %bitcast.29), kind=kOutput, calls=%fused_computation.15 | convolution fusion | flops 100663296 | bytes 16900096 | tf_op jit(solution)/shard_map/dot_general | solution.py:598
  36.2 0.1 collective-permute-start.10
  36.3 1.2 %collective-permute-done.10 = bf16[4,6,512]{2,1,0:T(8,128)(2,1)S(1)} collective-permute-done((bf16[4,6,512]{2,1,0:T(8,128)(2,1)S(1)}, bf16[4,6,512]{2,1,0:T(8,128)(2,1)S(1)}, u32[]{:S(2)}, u32[]{:S(2)}) %collective-permute-start.10) | collective-permute-done | bytes 24608 | tf_op jit(solution)/shard_map/ppermute | solution.py:490
  37.5 1.1 %collective-permute-start.11 = (bf16[6,512]{1,0:T(8,128)(2,1)S(1)}, bf16[6,512]{1,0:T(8,128)(2,1)S(1)}, u32[]{:S(2)}, u32[]{:S(2)}) collective-permute-start(bf16[6,512]{1,0:T(8,128)(2,1)S(1)} %get-tuple-element.21), channel_id=1, source_target_pairs={{0,2},{2,0},{4,6},{6,4},{1,3},{3,1},{5,7},{7,5},{8,10},{10,8},{12,... | collective-permute-start | bytes 18440 | tf_op jit(solution)/shard_map/ppermute | solution.py:490
  38.6 2.4 %collective-permute-start.13 = (bf16[6,512]{1,0:T(8,128)(2,1)S(1)}, bf16[6,512]{1,0:T(8,128)(2,1)S(1)}, u32[]{:S(2)}, u32[]{:S(2)}) collective-permute-start(bf16[6,512]{1,0:T(8,128)(2,1)S(1)} %get-tuple-element.22), channel_id=1, source_target_pairs={{0,6},{2,4},{4,2},{6,0},{1,7},{3,5},{5,3},{7,1},{8,14},{10,12},{12... | collective-permute-start | bytes 18440 | tf_op jit(solution)/shard_map/ppermute | solution.py:490
  41.0 0.1 collective-permute-start.12
  41.1 0.2 collective-permute-done.11
  41.2 2.8 %collective-permute-done.13 = bf16[6,512]{1,0:T(8,128)(2,1)S(1)} collective-permute-done((bf16[6,512]{1,0:T(8,128)(2,1)S(1)}, bf16[6,512]{1,0:T(8,128)(2,1)S(1)}, u32[]{:S(2)}, u32[]{:S(2)}) %collective-permute-start.13) | collective-permute-done | bytes 6176 | tf_op jit(solution)/shard_map/ppermute | solution.py:490
  44.0 1.5 %collective-permute-done.12 = bf16[6,512]{1,0:T(8,128)(2,1)S(1)} collective-permute-done((bf16[6,512]{1,0:T(8,128)(2,1)S(1)}, bf16[6,512]{1,0:T(8,128)(2,1)S(1)}, u32[]{:S(2)}, u32[]{:S(2)}) %collective-permute-start.12) | collective-permute-done | bytes 6176 | tf_op jit(solution)/shard_map/ppermute | solution.py:490
  45.5 0.6 %fusion.5 = bf16[6,512]{1,0:T(8,128)(2,1)} fusion(f32[4,6,512]{2,1,0:T(8,128)S(1)} %get-tuple-element.20, bf16[6,512]{1,0:T(8,128)(2,1)S(1)} %collective-permute-done.13, bf16[6,512]{1,0:T(8,128)(2,1)S(1)} %collective-permute-done.12, bf16[6,512]{1,0:T(8,128)(2,1)S(1)} %collective-permute-done.11), kind=kLoop, calls=%fused_computation.10 | loop fusion | flops 21504 | bytes 36864 | tf_op jit(solution)/shard_map/convert_element_type | solution.py:617
  (21 shorter events, 0.1 us)
Async XLA Ops:
  2.9 10.0 %copy-start.1 = (s32[6]{0:T(128)S(1)}, s32[6]{0:T(128)}, u32[]{:S(2)}) copy-start(s32[6]{0:T(128)} %lengths.1) | copy-start | bytes 76
  2.9 10.0 %copy-start.2 = (f32[2]{0:T(128)S(1)}, f32[2]{0:T(128)}, u32[]{:S(2)}) copy-start(f32[2]{0:T(128)} %offset.1) | copy-start | bytes 28
  2.9 7.0 %collective-permute-start.2 = (bf16[120,128]{1,0:T(8,128)(2,1)S(1)}, bf16[120,128]{1,0:T(8,128)(2,1)S(1)}, u32[]{:S(2)}, u32[]{:S(2)}) collective-permute-start(bf16[120,128]{1,0:T(8,128)(2,1)S(1)} %project.1.refs_0_), channel_id=1, source_target_pairs={{0,6},{2,4},{4,2},{6,0},{1,7},{3,5},{5,3},{7,1},{8,14},{10,12},{12... | collective-permute-start | bytes 92168 | tf_op jit(solution)/shard_map/ppermute | solution.py:490
  8.1 4.8 %collective-permute-start.1 = (bf16[120,128]{1,0:T(8,128)(2,1)S(1)}, bf16[120,128]{1,0:T(8,128)(2,1)S(1)}, u32[]{:S(2)}, u32[]{:S(2)}) collective-permute-start(bf16[120,128]{1,0:T(8,128)(2,1)S(1)} %project.1.refs_0_), channel_id=1, source_target_pairs={{0,4},{2,6},{4,0},{6,2},{1,5},{3,7},{5,1},{7,3},{8,12},{10,14},{12... | collective-permute-start | bytes 92168 | tf_op jit(solution)/shard_map/ppermute | solution.py:490
  8.1 4.8 %collective-permute-start = (bf16[120,128]{1,0:T(8,128)(2,1)S(1)}, bf16[120,128]{1,0:T(8,128)(2,1)S(1)}, u32[]{:S(2)}, u32[]{:S(2)}) collective-permute-start(bf16[120,128]{1,0:T(8,128)(2,1)S(1)} %project.1.refs_0_), channel_id=1, source_target_pairs={{0,2},{2,0},{4,6},{6,4},{1,3},{3,1},{5,7},{7,5},{8,10},{10,8},{12,... | collective-permute-start | bytes 92168 | tf_op jit(solution)/shard_map/ppermute | solution.py:490
  12.9 18.6 %slice-start = ((s8[16777216]{0:T(1024)(128)(4,1)}), s8[4194304]{0:T(1024)(128)(4,1)S(1)}, s32[]{:S(2)}) async-start(s8[16777216]{0:T(1024)(128)(4,1)} %bitcast.26), calls=%async_computation | async-start | bytes 8388608
  12.9 18.6 %slice-start.1 = ((s8[16777216]{0:T(1024)(128)(4,1)}), s8[4194304]{0:T(1024)(128)(4,1)S(1)}, s32[]{:S(2)}) async-start(s8[16777216]{0:T(1024)(128)(4,1)} %bitcast.26), calls=%async_computation.1 | async-start | bytes 8388608
  15.3 7.0 %copy-start.3 = (bf16[2048,1024]{1,0:T(8,128)(2,1)S(1)}, bf16[2048,1024]{1,0:T(8,128)(2,1)}, u32[]{:S(2)}) copy-start(bf16[2048,1024]{1,0:T(8,128)(2,1)} %param.26) | copy-start | bytes 12582916
  15.3 8.8 %copy-start.4 = (bf16[6,1024]{1,0:T(8,128)(2,1)S(1)}, bf16[6,1024]{1,0:T(8,128)(2,1)}, u32[]{:S(2)}) copy-start(bf16[6,1024]{1,0:T(8,128)(2,1)} %tokens_hbm.1) | copy-start | bytes 36868
  15.3 16.0 %copy-start = (f32[4096]{0:T(1024)S(1)}, f32[4096]{0:T(1024)}, u32[]{:S(2)}) copy-start(f32[4096]{0:T(1024)} %param.27) | copy-start | bytes 49156
  15.4 16.2 %slice-start.2 = ((s8[16777216]{0:T(1024)(128)(4,1)}), s8[4194304]{0:T(1024)(128)(4,1)S(1)}, s32[]{:S(2)}) async-start(s8[16777216]{0:T(1024)(128)(4,1)} %bitcast.26), calls=%async_computation.2 | async-start | bytes 8388608
  15.4 16.2 %slice-start.3 = ((s8[16777216]{0:T(1024)(128)(4,1)}), s8[4194304]{0:T(1024)(128)(4,1)S(1)}, s32[]{:S(2)}) async-start(s8[16777216]{0:T(1024)(128)(4,1)} %bitcast.26), calls=%async_computation.3 | async-start | bytes 8388608
  15.4 5.7 %collective-permute-start.5 = (bf16[112,128]{1,0:T(8,128)(2,1)S(1)}, bf16[112,128]{1,0:T(8,128)(2,1)S(1)}, u32[]{:S(2)}, u32[]{:S(2)}) collective-permute-start(bf16[112,128]{1,0:T(8,128)(2,1)S(1)} %attend.1.refs_0_), channel_id=1, source_target_pairs={{0,6},{2,4},{4,2},{6,0},{1,7},{3,5},{5,3},{7,1},{8,14},{10,12},{12... | collective-permute-start | bytes 86024 | tf_op jit(solution)/shard_map/ppermute | solution.py:490
  16.9 4.8 %collective-permute-start.4 = (bf16[112,128]{1,0:T(8,128)(2,1)S(1)}, bf16[112,128]{1,0:T(8,128)(2,1)S(1)}, u32[]{:S(2)}, u32[]{:S(2)}) collective-permute-start(bf16[112,128]{1,0:T(8,128)(2,1)S(1)} %attend.1.refs_0_), channel_id=1, source_target_pairs={{0,4},{2,6},{4,0},{6,2},{1,5},{3,7},{5,1},{7,3},{8,12},{10,14},{12... | collective-permute-start | bytes 86024 | tf_op jit(solution)/shard_map/ppermute | solution.py:490
  17.5 4.4 %collective-permute-start.3 = (bf16[112,128]{1,0:T(8,128)(2,1)S(1)}, bf16[112,128]{1,0:T(8,128)(2,1)S(1)}, u32[]{:S(2)}, u32[]{:S(2)}) collective-permute-start(bf16[112,128]{1,0:T(8,128)(2,1)S(1)} %attend.1.refs_0_), channel_id=1, source_target_pairs={{0,2},{2,0},{4,6},{6,4},{1,3},{3,1},{5,7},{7,5},{8,10},{10,8},{12,... | collective-permute-start | bytes 86024 | tf_op jit(solution)/shard_map/ppermute | solution.py:490
  22.0 11.9 %slice-start.4 = ((s8[16777216]{0:T(1024)(128)(4,1)}), s8[4194304]{0:T(1024)(128)(4,1)S(1)}, s32[]{:S(2)}) async-start(s8[16777216]{0:T(1024)(128)(4,1)} %bitcast.28), calls=%async_computation.4 | async-start | bytes 8388608
  22.0 11.9 %slice-start.5 = ((s8[16777216]{0:T(1024)(128)(4,1)}), s8[4194304]{0:T(1024)(128)(4,1)S(1)}, s32[]{:S(2)}) async-start(s8[16777216]{0:T(1024)(128)(4,1)} %bitcast.28), calls=%async_computation.5 | async-start | bytes 8388608
  22.0 11.9 %slice-start.6 = ((s8[16777216]{0:T(1024)(128)(4,1)}), s8[4194304]{0:T(1024)(128)(4,1)S(1)}, s32[]{:S(2)}) async-start(s8[16777216]{0:T(1024)(128)(4,1)} %bitcast.28), calls=%async_computation.6 | async-start | bytes 8388608
  23.0 1.2 %collective-permute-start.6 = (bf16[6,1024]{1,0:T(8,128)(2,1)S(1)}, bf16[6,1024]{1,0:T(8,128)(2,1)S(1)}, u32[]{:S(2)}, u32[]{:S(2)}) collective-permute-start(bf16[6,1024]{1,0:T(8,128)(2,1)S(1)} %convolution_convert_fusion), channel_id=1, source_target_pairs={{0,1},{1,0},{2,3},{3,2},{4,5},{5,4},{6,7},{7,6},{8,9},{9,8},{10,11... | collective-permute-start | bytes 36872 | tf_op jit(solution)/shard_map/ppermute | solution.py:490
  24.2 5.6 %collective-permute-start.9 = (bf16[6,1024]{1,0:T(8,128)(2,1)S(1)}, bf16[6,1024]{1,0:T(8,128)(2,1)S(1)}, u32[]{:S(2)}, u32[]{:S(2)}) collective-permute-start(bf16[6,1024]{1,0:T(8,128)(2,1)S(1)} %add_convert_fusion.refs_0_), channel_id=1, source_target_pairs={{0,6},{2,4},{4,2},{6,0},{1,7},{3,5},{5,3},{7,1},{8,14},{10,12},{12... | collective-permute-start | bytes 36872 | tf_op jit(solution)/shard_map/ppermute | solution.py:490
  26.6 4.7 %collective-permute-start.8 = (bf16[6,1024]{1,0:T(8,128)(2,1)S(1)}, bf16[6,1024]{1,0:T(8,128)(2,1)S(1)}, u32[]{:S(2)}, u32[]{:S(2)}) collective-permute-start(bf16[6,1024]{1,0:T(8,128)(2,1)S(1)} %add_convert_fusion.refs_0_), channel_id=1, source_target_pairs={{0,4},{2,6},{4,0},{6,2},{1,5},{3,7},{5,1},{7,3},{8,12},{10,14},{12... | collective-permute-start | bytes 36872 | tf_op jit(solution)/shard_map/ppermute | solution.py:490
  27.4 3.9 %collective-permute-start.7 = (bf16[6,1024]{1,0:T(8,128)(2,1)S(1)}, bf16[6,1024]{1,0:T(8,128)(2,1)S(1)}, u32[]{:S(2)}, u32[]{:S(2)}) collective-permute-start(bf16[6,1024]{1,0:T(8,128)(2,1)S(1)} %add_convert_fusion.refs_0_), channel_id=1, source_target_pairs={{0,2},{2,0},{4,6},{6,4},{1,3},{3,1},{5,7},{7,5},{8,10},{10,8},{12,... | collective-permute-start | bytes 36872 | tf_op jit(solution)/shard_map/ppermute | solution.py:490
  31.6 2.3 %slice-start.7 = ((s8[16777216]{0:T(1024)(128)(4,1)}), s8[4194304]{0:T(1024)(128)(4,1)S(1)}, s32[]{:S(2)}) async-start(s8[16777216]{0:T(1024)(128)(4,1)} %bitcast.28), calls=%async_computation.7 | async-start | bytes 8388608
  36.2 1.3 %collective-permute-start.10 = (bf16[4,6,512]{2,1,0:T(8,128)(2,1)S(1)}, bf16[4,6,512]{2,1,0:T(8,128)(2,1)S(1)}, u32[]{:S(2)}, u32[]{:S(2)}) collective-permute-start(bf16[4,6,512]{2,1,0:T(8,128)(2,1)S(1)} %get-tuple-element.18), channel_id=1, source_target_pairs={{0,1},{1,0},{2,3},{3,2},{4,5},{5,4},{6,7},{7,6},{8,9},{9,8},{10,11... | collective-permute-start | bytes 73736 | tf_op jit(solution)/shard_map/ppermute | solution.py:490
  37.5 3.7 %collective-permute-start.11 = (bf16[6,512]{1,0:T(8,128)(2,1)S(1)}, bf16[6,512]{1,0:T(8,128)(2,1)S(1)}, u32[]{:S(2)}, u32[]{:S(2)}) collective-permute-start(bf16[6,512]{1,0:T(8,128)(2,1)S(1)} %get-tuple-element.21), channel_id=1, source_target_pairs={{0,2},{2,0},{4,6},{6,4},{1,3},{3,1},{5,7},{7,5},{8,10},{10,8},{12,... | collective-permute-start | bytes 18440 | tf_op jit(solution)/shard_map/ppermute | solution.py:490
  38.6 5.4 %collective-permute-start.13 = (bf16[6,512]{1,0:T(8,128)(2,1)S(1)}, bf16[6,512]{1,0:T(8,128)(2,1)S(1)}, u32[]{:S(2)}, u32[]{:S(2)}) collective-permute-start(bf16[6,512]{1,0:T(8,128)(2,1)S(1)} %get-tuple-element.22), channel_id=1, source_target_pairs={{0,6},{2,4},{4,2},{6,0},{1,7},{3,5},{5,3},{7,1},{8,14},{10,12},{12... | collective-permute-start | bytes 18440 | tf_op jit(solution)/shard_map/ppermute | solution.py:490
  41.0 4.5 %collective-permute-start.12 = (bf16[6,512]{1,0:T(8,128)(2,1)S(1)}, bf16[6,512]{1,0:T(8,128)(2,1)S(1)}, u32[]{:S(2)}, u32[]{:S(2)}) collective-permute-start(bf16[6,512]{1,0:T(8,128)(2,1)S(1)} %get-tuple-element.23), channel_id=1, source_target_pairs={{0,4},{2,6},{4,0},{6,2},{1,5},{3,7},{5,1},{7,3},{8,12},{10,14},{12... | collective-permute-start | bytes 18440 | tf_op jit(solution)/shard_map/ppermute | solution.py:490
